TPU v7x, 32 devices: a whole 2x2x4 slice. The times are simulated.
32 devices in a mesh: sp: 8 (over z, y), tp: 4 (over x, core).
Axes of the slice: x: 2, y: 2, z: 4, core: 2. Of those that a mesh axis runs over, the one named last changes fastest.
Arguments:
- latent: bfloat16 [4096, 2048], P(('sp', 'tp')), may hold values from -6 to 6
- context: bfloat16 [512, 2048], P('sp'), may hold values from -6 to 6
- condition: float32 [2048], replicated, may hold values from -6 to 6
- context_condition: float32 [2048], replicated, may hold values from -6 to 6
- norm_gain: float32 [2048], replicated, may hold values from 0.1 to 1.9
- shift_weight: bfloat16 [2048, 2048], P('sp', 'tp'), may hold values from -0.21875 to 0.21875
- scale_weight: bfloat16 [2048, 2048], P('sp', 'tp'), may hold values from -0.21875 to 0.21875
- gate_weight: bfloat16 [2048, 2048], P('sp', 'tp'), may hold values from -0.21875 to 0.21875
- query_weight: bfloat16 [2048, 1024], P(None, 'tp'), may hold values from -1 to 1
- key_weight: bfloat16 [2048, 512], P(None, 'tp'), may hold values from -1 to 1
- value_weight: bfloat16 [2048, 512], P(None, 'tp'), may hold values from -0.125 to 0.125
- query_gain: float32 [64], replicated, may hold values from 0.1 to 7.8
- key_gain: float32 [64], replicated, may hold values from 0.1 to 7.8
- output_weight: bfloat16 [1024, 2048], replicated, may hold values from -1 to 1
Outputs:
- updated: bfloat16 [4096, 2048], P(('sp', 'tp'))
All inputs are finite; a program needn't handle non-finite values.
Results may differ from a plain program's by a relative error of at most 0.012.
The roundings to bfloat16 on the way count: a program that leaves them out, or rounds other values in their place, can miss the bound.
Values may be sent and summed in bfloat16 or wider, within the bound.
A program may use at most 64 MiB of HBM per device.

v0:
```python
import functools
import math

import jax
import jax.numpy as jnp
from jax import lax
from jax.experimental import pallas as pl
from jax.experimental.pallas import tpu as pltpu
from jax.sharding import PartitionSpec as P

CHANNEL_SPAN = 64
GRID_W = 64
TILE = 512
UNROLL = 4
MESH = pl.DeviceIdType.MESH
VMEM = pl.BlockSpec(memory_space=pltpu.VMEM)
F32 = jnp.float32
BF16 = jnp.bfloat16

epsilon = 1e-06
rope_base = 10000.0


def greet(n_sp, n_tp):
    sp, tp = lax.axis_index("sp"), lax.axis_index("tp")
    barrier = pltpu.get_barrier_semaphore()
    for d in range(1, n_sp):
        pl.semaphore_signal(
            barrier, inc=1, device_id=(lax.rem(sp + d, n_sp), tp), device_id_type=MESH
        )
    for d in range(1, n_tp):
        pl.semaphore_signal(
            barrier, inc=1, device_id=(sp, lax.rem(tp + d, n_tp)), device_id_type=MESH
        )
    pl.semaphore_wait(barrier, n_sp + n_tp - 2)


def gather_kernel(
    n_sp, n_tp, latent_hbm, act, w_shift_hbm, w_scale_hbm, w_gate_hbm, context_hbm, norm_gain,
    w_q_hbm, w_k_hbm, w_v_hbm, q_gain, k_gain, inverse, q_out, kv_out, mods,
    lat_all, w_mod, context, w_q, w_k, w_v, hidden, part, parts,
    cosine, sine, load, lat_send, lat_recv, fwd_send, sp_send, sp_recv, tp_send, tp_recv,
):
    sp, tp = lax.axis_index("sp"), lax.axis_index("tp")
    loads = [
        pltpu.make_async_copy(src, dst, load.at[i])
        for i, (src, dst) in enumerate(
            (
                (w_shift_hbm, w_mod.at[0]), (w_scale_hbm, w_mod.at[1]), (w_gate_hbm, w_mod.at[2]),
                (latent_hbm, lat_all.at[tp]), (context_hbm, context),
                (w_k_hbm, w_k), (w_v_hbm, w_v), (w_q_hbm, w_q),
            )
        )
    ]
    loads[3].start()
    for i, c in enumerate(loads):
        if i != 3:
            c.start()
    greet(n_sp, n_tp)
    core = lax.rem(tp, 2)
    twin = tp + 1 - 2 * core
    chips = n_tp // 2

    def row_copy(src, send_sem, peer):
        return pltpu.make_async_remote_copy(
            src_ref=lat_all.at[src], dst_ref=lat_all.at[src], send_sem=send_sem,
            recv_sem=lat_recv.at[src], device_id=(sp, peer), device_id_type=MESH,
        )

    loads[3].wait()
    sends = []
    for d in range(1, chips):
        sends.append(row_copy(tp, lat_send.at[d], lax.rem(tp + 2 * d, n_tp)))
    sends.append(row_copy(tp, lat_send.at[0], twin))
    for c in sends:
        c.start()
    part[...] = jnp.zeros_like(part)
    for i in range(3):
        loads[i].wait()
        part[2 * i : 2 * i + 2, :] = jnp.dot(act[...], w_mod[i], preferred_element_type=F32)
    sp_copies = []
    for d in range(1, n_sp):
        c = pltpu.make_async_remote_copy(
            src_ref=part, dst_ref=parts.at[sp], send_sem=sp_send.at[d - 1],
            recv_sem=sp_recv.at[d - 1], device_id=(lax.rem(sp + d, n_sp), tp), device_id_type=MESH,
        )
        c.start()
        sp_copies.append(c)
    parts[sp] = part[...]
    tok = cosine.shape[0]
    place = sp * tok + lax.broadcasted_iota(jnp.int32, (tok, 128), 0)
    lane = lax.broadcasted_iota(jnp.int32, (tok, 128), 1) % CHANNEL_SPAN
    coord = jnp.where(lane < CHANNEL_SPAN // 2, place // GRID_W, place % GRID_W)
    angles = coord.astype(F32) * inverse[...]
    cosine[...] = jnp.cos(angles)
    turn = jnp.sin(angles)
    sine[...] = jnp.where(lane % (CHANNEL_SPAN // 2) < CHANNEL_SPAN // 4, -turn, turn)
    for c in sp_copies:
        c.wait()
    total = parts[0]
    for j in range(1, n_sp):
        total = total + parts[j]
    part[...] = total
    mods[tp] = total
    tp_copies = []
    for d in range(1, n_tp):
        c = pltpu.make_async_remote_copy(
            src_ref=part, dst_ref=mods.at[tp], send_sem=tp_send.at[d - 1],
            recv_sem=tp_recv.at[d - 1], device_id=(sp, lax.rem(tp + d, n_tp)), device_id_type=MESH,
        )
        c.start()
        tp_copies.append(c)
    for c in loads[4:]:
        c.wait()
    for c in tp_copies:
        c.wait()
    context_step, tile = project(
        n_tp, lat_all, context, mods, norm_gain, w_q, w_k, w_v, q_gain, k_gain, cosine, sine,
        q_out, kv_out, hidden,
    )
    context_step()
    tile(tp)
    forwards = []
    for d in range(1, chips):
        src = lax.rem(tp - 2 * d + n_tp, n_tp)
        row_copy(src, lat_send.at[0], twin).wait_recv()
        c = row_copy(src, fwd_send.at[d - 1], twin)
        c.start()
        forwards.append(c)
    row_copy(twin, lat_send.at[0], twin).wait_recv()
    tile(twin)
    for d in range(1, chips):
        tile(lax.rem(tp - 2 * d + n_tp, n_tp))
    for d in range(1, chips):
        src = lax.rem(twin - 2 * d + n_tp, n_tp)
        row_copy(src, lat_send.at[0], twin).wait_recv()
        tile(src)
    for c in sends + forwards:
        c.wait_send()


def project(
    n_tp, lat_all, context, mods, norm_gain, w_q, w_k, w_v, q_gain, k_gain, cosine, sine,
    q_out, kv_out, hidden,
):
    own_rows = lat_all.shape[1]
    ctx_rows = context.shape[0]
    q_width = w_q.shape[1]
    kv_width = w_k.shape[1]
    kv_heads = kv_width // CHANNEL_SPAN
    q_heads = q_width // CHANNEL_SPAN
    group = q_heads // kv_heads
    span = mods.shape[2]

    def modulate(read, rows, row):
        total = jnp.zeros((rows, 1), F32)
        for t in range(n_tp):
            x = read(t).astype(F32)
            total = total + jnp.sum(x * x, axis=-1, keepdims=True)
        inv = lax.rsqrt(total / (n_tp * span) + epsilon)
        for t in range(n_tp):
            cols = slice(t * span, (t + 1) * span)
            x = read(t).astype(F32)
            y = x * inv * norm_gain[:, cols] * (1.0 + mods[t, 2 + row : 3 + row, :]) + mods[
                t, row : row + 1, :
            ]
            hidden[0:rows, cols] = y.astype(BF16)

    def headnorm(x, gain):
        width = x.shape[1]
        head = lax.broadcasted_iota(jnp.int32, x.shape, 1) // CHANNEL_SPAN
        sq = x * x
        scale = jnp.zeros_like(x)
        for h in range(width // CHANNEL_SPAN):
            s = jnp.sum(jnp.where(head == h, sq, 0.0), axis=-1, keepdims=True)
            scale = jnp.where(head == h, lax.rsqrt(s / CHANNEL_SPAN + epsilon), scale)
        return x * scale * gain

    def rotate(x, cos, sin):
        width = x.shape[1]
        full = x if width == 128 else jnp.concatenate([x, x], axis=1)
        lane = lax.broadcasted_iota(jnp.int32, full.shape, 1)
        other = jnp.where(lane % 32 < 16, pltpu.roll(full, 112, 1), pltpu.roll(full, 16, 1))
        return (full * cos + other * sin)[:, :width]

    piece = min(128, kv_width)
    q_pair = jnp.concatenate([q_gain[...], q_gain[...]], axis=1)
    k_pair = jnp.concatenate([k_gain[...], k_gain[...]], axis=1)

    def context_step():
        modulate(lambda t: context[:, t * span : (t + 1) * span], ctx_rows, 1)
        h = hidden[0:ctx_rows, :]
        k = jnp.dot(h, w_k[...], preferred_element_type=F32)
        for c in range(0, kv_width, piece):
            kv_out[0:ctx_rows, c : c + piece] = headnorm(
                k[:, c : c + piece], k_pair[:, :piece]
            ).astype(BF16)
        kv_out[0:ctx_rows, kv_width:] = jnp.dot(h, w_v[...], preferred_element_type=F32).astype(
            BF16
        )

    def tile(i):
        modulate(lambda t: lat_all[i, :, t * span : (t + 1) * span], own_rows, 0)
        h = hidden[0:own_rows, :]
        rows = pl.ds(pl.multiple_of(i * own_rows, own_rows), own_rows)
        cos, sin = cosine[rows, :], sine[rows, :]
        low = pl.ds(pl.multiple_of(ctx_rows + i * own_rows, 16), own_rows)
        k = jnp.dot(h, w_k[...], preferred_element_type=F32)
        for c in range(0, kv_width, piece):
            kv_out[low, c : c + piece] = rotate(
                headnorm(k[:, c : c + piece], k_pair[:, :piece]), cos, sin
            ).astype(BF16)
        kv_out[low, kv_width:] = jnp.dot(h, w_v[...], preferred_element_type=F32).astype(BF16)
        q = jnp.dot(h, w_q[...], preferred_element_type=F32)
        for c in range(0, q_width, 128):
            y = rotate(headnorm(q[:, c : c + 128], q_pair), cos, sin).astype(BF16)
            y = y.astype(F32) * CHANNEL_SPAN ** (-0.5)
            lane = lax.broadcasted_iota(jnp.int32, y.shape, 1)
            for j in range(2):
                head = c // CHANNEL_SPAN + j
                place = head // group
                moved = y if place % 2 == j else pltpu.roll(y, 64, 1)
                base = place // 2 * 128
                inside = lane // CHANNEL_SPAN == place % 2
                blank = jnp.where(inside, moved, 0.0).astype(BF16)
                for b in range(0, kv_width, piece):
                    q_out[head, rows, b : b + piece] = (
                        blank[:, :piece] if b == base else jnp.zeros((own_rows, piece), BF16)
                    )

    return context_step, tile


def attend_kernel(
    n_sp, n_tp, lows, tile_rows, unroll, ctx_rows, offset, q, kv, mods, latent_hbm, w_out_hbm, out,
    kv_all, peak, total, acc, attended, received, latent, w_out,
    lo_send, hi_send, fwd_send, kv_recv, at_send, at_recv, own_sem, lat_sem, w_sem,
):
    sp, tp = lax.axis_index("sp"), lax.axis_index("tp")
    tok, width2 = q.shape[1], kv.shape[1]
    width = width2 // 2
    kv_heads = width // CHANNEL_SPAN
    q_heads = q.shape[0]
    group = q_heads // kv_heads
    own_rows = tok // n_tp
    q_width = q_heads * CHANNEL_SPAN
    fetch = pltpu.make_async_copy(w_out_hbm, w_out, w_sem)
    fetch_latent = pltpu.make_async_copy(latent_hbm, latent, lat_sem)
    greet(n_sp, n_tp)
    highs = n_sp // lows
    low, high = lax.rem(sp, lows), sp // lows

    def copy(src, slot, send_sem, peer):
        return pltpu.make_async_remote_copy(
            src_ref=slot, dst_ref=kv_all.at[src], send_sem=send_sem,
            recv_sem=kv_recv.at[src], device_id=(peer, tp), device_id_type=MESH,
        )

    def low_peer(d):
        return high * lows + lax.rem(low + d, lows)

    def high_peer(d):
        return lax.rem(high + d, highs) * lows + low

    sends = [copy(sp, kv, lo_send.at[d - 1], low_peer(d)) for d in range(1, lows)]
    sends += [copy(sp, kv, hi_send.at[d - 1], high_peer(d)) for d in range(1, highs)]
    for c in sends:
        c.start()
    own = pltpu.make_async_copy(kv, kv_all.at[sp], own_sem)
    own.start()
    fetch.start()
    fetch_latent.start()
    tiles = tok // tile_rows

    def update(keys, values, shift, first):
        def step(i, carry):
            head, r = i // tiles, lax.rem(i, tiles)
            rows = pl.ds(pl.multiple_of(r * tile_rows, tile_rows), tile_rows)
            s = lax.dot_general(
                q[head, rows, :], keys(), (((1,), (1,)), ((), ())), preferred_element_type=F32
            )
            if shift:
                s = s + shift
            top = jnp.max(s, axis=-1, keepdims=True)
            if not first:
                old = peak[head, rows, 0:1]
                top = jnp.maximum(top, old)
                shrink = jnp.exp(old - top)
            e = jnp.exp(s - top)
            row_sum = e[:, 0:128]
            for c in range(128, e.shape[1], 128):
                row_sum = row_sum + e[:, c : c + 128]
            w = jnp.dot(e.astype(BF16), values(), preferred_element_type=F32)
            if not first:
                row_sum = row_sum + total[head, rows, :] * shrink
                w = w + acc[head, rows, :] * shrink
            peak[head, rows, :] = jnp.broadcast_to(top, (tile_rows, 128))
            total[head, rows, :] = row_sum
            acc[head, rows, :] = w
            return carry

        lax.fori_loop(0, q_heads * tiles, step, 0, unroll=unroll)

    def attend(src):
        update(
            lambda: kv_all[src, ctx_rows:, :width], lambda: kv_all[src, ctx_rows:, width:],
            0.0, False,
        )

    def arrive(src):
        copy(src, kv, lo_send.at[0], low_peer(0)).wait_recv()

    update(lambda: kv[ctx_rows:, :width], lambda: kv[ctx_rows:, width:], 0.0, True)

    def near(d, carry):
        src = high * lows + lax.rem(low - d + lows, lows)
        arrive(src)
        attend(src)
        return carry

    lax.fori_loop(1, lows, near, 0)

    def column(d, carry):
        row = lax.rem(high - d + highs, highs) * lows
        src = row + low
        arrive(src)

        def pass_on(e, inner):
            copy(
                src, kv_all.at[src], fwd_send.at[(d - 1) * (lows - 1) + e - 1], low_peer(e)
            ).start()
            return inner

        lax.fori_loop(1, lows, pass_on, 0)
        attend(src)
        return carry

    lax.fori_loop(1, highs, column, 0)

    def rest(k, carry):
        d, e = k // (lows - 1) + 1, lax.rem(k, lows - 1) + 1
        src = lax.rem(high - d + highs, highs) * lows + lax.rem(low - e + lows, lows)
        arrive(src)
        attend(src)
        return carry

    lax.fori_loop(0, (highs - 1) * (lows - 1), rest, 0)
    own.wait()
    ctx_count = n_sp * ctx_rows
    update(
        lambda: kv_all[:, :ctx_rows, :width].reshape(ctx_count, width),
        lambda: kv_all[:, :ctx_rows, width:].reshape(ctx_count, width),
        offset,
        False,
    )
    for c in sends:
        c.wait_send()

    def sent(k, carry):
        copy(sp, kv, fwd_send.at[k], low_peer(1)).wait_send()
        return carry

    lax.fori_loop(0, (highs - 1) * (lows - 1), sent, 0)
    for t in range(n_tp):
        rows = slice(t * own_rows, (t + 1) * own_rows)
        for h in range(q_heads):
            g = h // group
            a = acc[h, rows, :] / jnp.sum(total[h, rows, :], axis=-1, keepdims=True)
            attended[t, :, h * CHANNEL_SPAN : (h + 1) * CHANNEL_SPAN] = a[
                :, g * CHANNEL_SPAN : (g + 1) * CHANNEL_SPAN
            ].astype(BF16)
    copies = []
    for d in range(1, n_tp):
        peer = lax.rem(tp + d, n_tp)
        c = pltpu.make_async_remote_copy(
            src_ref=attended.at[peer], dst_ref=received.at[tp], send_sem=at_send.at[d - 1],
            recv_sem=at_recv.at[d - 1], device_id=(sp, peer), device_id_type=MESH,
        )
        c.start()
        copies.append(c)
    received[tp] = attended[tp]
    fetch.wait()
    fetch_latent.wait()
    for c in copies:
        c.wait()
    span = mods.shape[2]
    for t in range(n_tp):
        cols = slice(t * span, (t + 1) * span)
        branch = jnp.zeros((own_rows, span), F32)
        for s in range(n_tp):
            branch = branch + jnp.dot(
                received[s],
                w_out[s * q_width : (s + 1) * q_width, cols],
                preferred_element_type=F32,
            )
        out[:, cols] = (latent[:, cols].astype(F32) + mods[t, 4:5, :] * branch).astype(BF16)


def on_device(
    latent, context, condition, context_condition, norm_gain, shift_weight, scale_weight,
    gate_weight, query_weight, key_weight, value_weight, query_gain, key_gain, output_weight,
):
    n_sp, n_tp = lax.axis_size("sp"), lax.axis_size("tp")
    seq_index = lax.axis_index("sp")
    row_slab, columns = shift_weight.shape
    own_rows, model = latent.shape
    ctx_rows = context.shape[0]
    tok = own_rows * n_tp
    q_width, kv_width = query_weight.shape[1], key_weight.shape[1]
    q_heads = q_width // CHANNEL_SPAN
    conditions = jnp.stack([condition, context_condition])
    act = jax.nn.silu(
        lax.dynamic_slice_in_dim(conditions, seq_index * row_slab, row_slab, 1)
    ).astype(BF16)
    dma = pltpu.SemaphoreType.DMA
    quarter = CHANNEL_SPAN // 4
    lane = jnp.arange(128, dtype=jnp.int32) % CHANNEL_SPAN
    inverse = (rope_base ** (-(lane % quarter).astype(F32) / quarter))[None]
    anywhere = pl.BlockSpec(memory_space=pl.ANY)
    q, kv, mods = pl.pallas_call(
        functools.partial(gather_kernel, n_sp, n_tp),
        out_shape=(
            jax.ShapeDtypeStruct((q_heads, tok, kv_width), BF16),
            jax.ShapeDtypeStruct((ctx_rows + tok, 2 * kv_width), BF16),
            jax.ShapeDtypeStruct((n_tp, 8, columns), F32),
        ),
        in_specs=[anywhere, VMEM] + [anywhere] * 4 + [VMEM] + [anywhere] * 3 + [VMEM] * 3,
        out_specs=(VMEM, VMEM, VMEM),
        scratch_shapes=[
            pltpu.VMEM((n_tp, own_rows, model), BF16),
            pltpu.VMEM((3, row_slab, columns), BF16),
            pltpu.VMEM(context.shape, BF16),
            pltpu.VMEM(query_weight.shape, BF16),
            pltpu.VMEM(key_weight.shape, BF16),
            pltpu.VMEM(value_weight.shape, BF16),
            pltpu.VMEM((max(own_rows, ctx_rows), model), BF16),
            pltpu.VMEM((8, columns), F32),
            pltpu.VMEM((n_sp, 8, columns), F32),
            pltpu.VMEM((tok, 128), F32),
            pltpu.VMEM((tok, 128), F32),
            dma((8,)), dma((n_tp // 2,)), dma((n_tp,)), dma((max(n_tp // 2 - 1, 1),)),
            dma((n_sp - 1,)), dma((n_sp - 1,)), dma((n_tp - 1,)), dma((n_tp - 1,)),
        ],
        compiler_params=pltpu.CompilerParams(
            collective_id=0, has_side_effects=True, vmem_limit_bytes=56 << 20
        ),
        name="gather_project",
    )(
        latent, act, shift_weight, scale_weight, gate_weight, context, norm_gain[None],
        query_weight, key_weight, value_weight,
        query_gain[None], key_gain[None], inverse,
    )
    offset = math.log(tok / (2.0 * ctx_rows))
    tile_rows = math.gcd(tok, TILE)
    lows = 2 ** (int(math.log2(n_sp)) // 2)
    return pl.pallas_call(
        functools.partial(
            attend_kernel, n_sp, n_tp, lows, tile_rows, UNROLL, ctx_rows, offset
        ),
        out_shape=jax.ShapeDtypeStruct(latent.shape, BF16),
        in_specs=[VMEM] * 3 + [anywhere] * 2,
        out_specs=VMEM,
        scratch_shapes=[
            pltpu.VMEM((n_sp, ctx_rows + tok, 2 * kv_width), BF16),
            pltpu.VMEM((q_heads, tok, 128), F32),
            pltpu.VMEM((q_heads, tok, 128), F32),
            pltpu.VMEM((q_heads, tok, kv_width), F32),
            pltpu.VMEM((n_tp, own_rows, q_width), BF16),
            pltpu.VMEM((n_tp, own_rows, q_width), BF16),
            pltpu.VMEM(latent.shape, BF16),
            pltpu.VMEM(output_weight.shape, BF16),
            dma((lows - 1,)), dma((n_sp // lows - 1,)),
            dma(((n_sp // lows - 1) * (lows - 1),)), dma((n_sp,)),
            dma((n_tp - 1,)), dma((n_tp - 1,)), dma, dma, dma,
        ],
        compiler_params=pltpu.CompilerParams(
            collective_id=1, has_side_effects=True, vmem_limit_bytes=56 << 20
        ),
        name="attend",
    )(q, kv, mods, latent, output_weight)


def solution(mesh):
    in_specs = (
        P(("sp", "tp"), None), P("sp", None), P(), P(), P(),
        P("sp", "tp"), P("sp", "tp"), P("sp", "tp"),
        P(None, "tp"), P(None, "tp"), P(None, "tp"), P(), P(), P(),
    )
    return jax.shard_map(
        on_device, mesh=mesh, in_specs=in_specs, out_specs=P(("sp", "tp"), None), check_vma=False
    )
```

profile of v0, /device:TPU:25, one launch (start us, length us, event | category | flops | bytes accessed | tf_op | source)
XLA Modules:
  0.0 81.9 jit_solution(6193027387454305997)
XLA Ops:
  0.0 1.3 %fusion.1.act = bf16[2,256]{1,0:T(2,128)(2,1)} fusion(s32[]{:T(128)S(6)} %select_n.28, f32[1,2048]{1,0:T(1,128)} %bitcast.6, f32[1,2048]{1,0:T(1,128)} %bitcast.7), kind=kLoop, calls=%fused_computation.6 | loop fusion | flops 3072 | bytes 17412 | tf_op jit(solution)/shard_map/convert_element_type | solution.py:414
  1.4 0.5 fusion.5.inverse
  1.9 21.5 %gather_project.1 = (bf16[4,512,128]{2,1,0:T(8,128)(2,1)}, bf16[576,256]{1,0:T(8,128)(2,1)}, f32[4,8,512]{2,1,0:T(8,128)}) custom-call(bf16[128,2048]{1,0:T(8,128)(2,1)} %latent_hbm.3, bf16[2,256]{1,0:T(2,128)(2,1)} %fusion.1.act, bf16[256,512]{1,0:T(8,128)(2,1)} %w_shift_hbm.1, bf16[256,512]{1,0:T(8,128)(2,1)} %w_scale_hbm.1, bf16[256,512]{1,0:T(8,128)(2,1)} %w_gate_hbm.1, ...), custom_call_target="tpu_custom_call" | custom-call | tf_op jit(solution)/shard_map/gather_project/pallas_call | solution.py:420
  23.3 56.6 %attend.1 = bf16[128,2048]{1,0:T(8,128)(2,1)} custom-call(bf16[4,512,128]{2,1,0:T(8,128)(2,1)} %get-tuple-element.8.q, bf16[576,256]{1,0:T(8,128)(2,1)} %get-tuple-element.9.kv, f32[4,8,512]{2,1,0:T(8,128)} %get-tuple-element.10.mods, bf16[128,2048]{1,0:T(8,128)(2,1)} %latent_hbm.3, bf16[1024,2048]{1,0:T(8,128)(2,1)} %w_out_hbm.1), custom_call_target="tpu_custom_call" | custom-call | tf_op jit(solution)/shard_map/attend/pallas_call | solution.py:456
  80.0 1.9 %copy.16 = bf16[128,2048]{1,0:T(8,128)(2,1)} copy(bf16[128,2048]{1,0:T(8,128)(2,1)} %attend.1) | data formatting | bytes 1048576
where the time goes:
time: 82.1 us; the launch traced here: 81.9 us
  Pallas kernels  78.1 us (95%)
  local copies, waits for them, and re-layouts  1.88 us (2%)
  other arithmetic  1.86 us (2%)
    pallas_call x1, Pallas kernels, on_device(): pl.pallas_call(functools.partial(attend_kernel, n_sp, n_tp, lows, tile_ro...  56.6 us
    pallas_call x1, Pallas kernels, on_device(): pl.pallas_call(functools.partial(gather_kernel, n_sp, n_tp), out_shape=(j...  21.5 us
    unnamed x1, local copies, waits for them, and re-layouts  1.88 us

commit v1 on v0

v1 whole, which is shorter than its diff:
```python
import functools
import math

import jax
import jax.numpy as jnp
from jax import lax
from jax.experimental import pallas as pl
from jax.experimental.pallas import tpu as pltpu
from jax.sharding import PartitionSpec as P

SPAN = 64
GRID_W = 64
QUARTER = SPAN // 4
LAG = 3
PIECES = 2
LOG2E = 1.4426950408889634
MESH = pl.DeviceIdType.MESH
VMEM = pl.BlockSpec(memory_space=pltpu.VMEM)
ANY = pl.BlockSpec(memory_space=pl.ANY)
F32 = jnp.float32
BF16 = jnp.bfloat16

epsilon = 1e-06
rope_base = 10000.0


def kernel(
    n_sp, n_tp, lows, offset,
    latent_hbm, context_hbm, cond, ctx_cond, norm_gain, w_shift_hbm, w_scale_hbm, w_gate_hbm,
    w_q_hbm, w_k_hbm, w_v_hbm, q_gain, k_gain, w_out_hbm,
    out,
    lat, context, w_mod, w_all, w_side, w_out, part, parts, mods, coef, hidden,
    table, gain_q, gain_k, q_send, kv_send, ctx_send, ctx_all, q_all, kv_all, k_nat,
    peak, total, acc, attended, received,
    load, lat_send, lat_fwd, lat_recv, sp_send, sp_recv, tp_send, tp_recv,
    q_ssem, q_rsem, z_send, y_send, f_send, kv_recv,
    cz_send, cy_send, cf_send, c_recv, at_send, at_recv,
):
    sp, tp = lax.axis_index("sp"), lax.axis_index("tp")
    chips = n_tp // 2
    highs = n_sp // lows
    low, high = lax.rem(sp, lows), sp // lows
    x, core = tp // 2, lax.rem(tp, 2)
    twin = tp + 1 - 2 * core
    width = lat.shape[1]
    own_rows = width // 2
    model = lat.shape[2]
    tok = chips * width
    ctx_rows = context.shape[0]
    groups = kv_send.shape[1]
    heads = q_send.shape[2]
    q_width = groups * heads * SPAN
    kv_width = groups * SPAN
    row_slab, columns = w_mod.shape[1], w_mod.shape[2]
    g = lax.rem(high, groups)
    base = high - g
    ctx_slots = n_sp * ctx_rows // width
    ctx_first = chips * n_sp

    def dev(z, y):
        return z * lows + y

    def remote(src, dst, ssem, rsem, peer):
        return pltpu.make_async_remote_copy(
            src_ref=src, dst_ref=dst, send_sem=ssem, recv_sem=rsem,
            device_id=peer, device_id_type=MESH,
        )

    def own_part(ref, chip, half):
        return ref.at[chip, pl.ds(pl.multiple_of(half * own_rows, own_rows), own_rows), :]

    pairs = [
        (latent_hbm, own_part(lat, x, core)),
        (w_shift_hbm, w_mod.at[0]), (w_scale_hbm, w_mod.at[1]), (w_gate_hbm, w_mod.at[2]),
        (context_hbm, context), (w_q_hbm, w_all.at[:, 0:q_width]),
    ]
    if kv_width % 128 == 0:
        pairs += [
            (w_k_hbm, w_all.at[:, q_width : q_width + kv_width]),
            (w_v_hbm, w_all.at[:, q_width + kv_width :]),
        ]
    else:
        pairs += [(w_k_hbm, w_side.at[0]), (w_v_hbm, w_side.at[1])]
    pairs.append((w_out_hbm, w_out))
    loads = [pltpu.make_async_copy(s, d, load.at[i]) for i, (s, d) in enumerate(pairs)]
    for c in loads:
        c.start()

    barrier = pltpu.get_barrier_semaphore()
    peers = [(lax.rem(sp + d, n_sp), tp) for d in range(1, n_sp)]
    peers += [(sp, lax.rem(tp + d, n_tp)) for d in range(1, n_tp)]
    for r in range(1, groups):
        mate = dev(base + lax.rem(g + r, groups), low)
        peers += [(mate, lax.rem(tp + d, n_tp)) for d in range(1, n_tp)]
    for p in peers:
        pl.semaphore_signal(barrier, inc=1, device_id=p, device_id_type=MESH)
    pl.semaphore_wait(barrier, len(peers))

    step = own_rows // PIECES

    def rows_of(tile, piece):
        chip, half = tile // 2, lax.rem(tile, 2)
        start = pl.multiple_of(half * own_rows + piece * step, step)
        return lat.at[chip, pl.ds(start, step), :]

    def row_copy(tile, piece, ssem, peer):
        return remote(
            rows_of(tile, piece), rows_of(tile, piece), ssem, lat_recv.at[tile, piece], (sp, peer)
        )

    lat_sends = []

    def send_piece(piece):
        for d in range(1, chips):
            c = row_copy(tp, piece, lat_send.at[d, piece], lax.rem(tp + 2 * d, n_tp))
            c.start()
            lat_sends.append(c)

    loads[0].wait()
    send_piece(0)
    for piece in range(PIECES):
        c = row_copy(tp, piece, lat_send.at[0, piece], twin)
        c.start()
        lat_sends.append(c)

    def slab(ref):
        if row_slab % 128 == 0:
            return ref[:, pl.ds(pl.multiple_of(sp * row_slab, 128), row_slab)]
        per = 128 // row_slab
        window = ref[:, pl.ds(pl.multiple_of(sp // per * 128, 128), 128)]
        pick = lax.rem(sp, per)
        result = window
        for k in range(1, per):
            result = jnp.where(pick == k, pltpu.roll(window, 128 - k * row_slab, 1), result)
        return result[:, :row_slab]

    v = jnp.concatenate([slab(cond), slab(ctx_cond)], axis=0)
    act = (v / (1.0 + jnp.exp(-v))).astype(BF16)
    part[...] = jnp.zeros_like(part)
    for i in range(3):
        loads[1 + i].wait()
        part[2 * i : 2 * i + 2, :] = jnp.dot(act, w_mod[i], preferred_element_type=F32)
    sp_copies = []
    for d in range(1, n_sp):
        c = remote(
            part, parts.at[sp], sp_send.at[d - 1], sp_recv.at[d - 1], (lax.rem(sp + d, n_sp), tp)
        )
        c.start()
        sp_copies.append(c)
    parts[sp] = part[...]

    for d in range(chips):
        chip = lax.rem(x - d + chips, chips)
        place = sp * tok + chip * width + lax.broadcasted_iota(jnp.int32, (QUARTER, width), 1)
        turn = lax.broadcasted_iota(jnp.int32, (QUARTER, width), 0).astype(F32)
        freq = jnp.exp(turn * (-math.log(rope_base) / QUARTER))
        by_row = (place // GRID_W).astype(F32) * freq
        by_col = (place % GRID_W).astype(F32) * freq
        table[d, 0:QUARTER, :] = jnp.cos(by_row)
        table[d, QUARTER : 2 * QUARTER, :] = jnp.sin(by_row)
        table[d, 2 * QUARTER : 3 * QUARTER, :] = jnp.cos(by_col)
        table[d, 3 * QUARTER :, :] = jnp.sin(by_col)
    k_pair = jnp.concatenate([k_gain[...], k_gain[...]], axis=1)
    for ref, dst in ((q_gain, gain_q), (k_gain, gain_k)):
        row = jnp.concatenate([ref[...], ref[...]], axis=1)
        square = jnp.transpose(jnp.broadcast_to(row, (128, 128)))[0:SPAN, :]
        for c in range(0, width, 128):
            dst[:, c : c + 128] = square
    peak[...] = jnp.full_like(peak, -1e30)
    total[...] = jnp.zeros_like(total)
    acc[...] = jnp.zeros_like(acc)
    q_all[:, :, SPAN:, :] = jnp.zeros((q_all.shape[0], heads, SPAN, width), BF16)

    for c in sp_copies:
        c.wait()
    summed = parts[0]
    for j in range(1, n_sp):
        summed = summed + parts[j]
    part[...] = summed
    mods[tp] = summed
    tp_copies = []
    for d in range(1, n_tp):
        c = remote(
            part, mods.at[tp], tp_send.at[d - 1], tp_recv.at[d - 1], (sp, lax.rem(tp + d, n_tp))
        )
        c.start()
        tp_copies.append(c)
    for piece in range(1, PIECES):
        send_piece(piece)
    for c in loads[4:-1]:
        c.wait()
    if kv_width % 128 != 0:
        w_all[:, q_width:] = jnp.concatenate([w_side[0], w_side[1]], axis=1)
    for piece in range(PIECES):
        row_copy(twin, piece, lat_send.at[0, 0], twin).wait_recv()
    for c in tp_copies:
        c.wait()
    for t in range(n_tp):
        cols = slice(t * columns, (t + 1) * columns)
        for row in range(2):
            coef[row : row + 1, cols] = norm_gain[:, cols] * (1.0 + mods[t, 2 + row : 3 + row, :])
            coef[2 + row : 3 + row, cols] = mods[t, row : row + 1, :]

    block = 16

    def modulate(read, rows, row):
        def body(i, carry):
            r = pl.ds(pl.multiple_of(i * block, block), block)
            w = read(r).astype(F32)
            inv = lax.rsqrt(jnp.sum(w * w, axis=-1, keepdims=True) / model + epsilon)
            y = w * inv * coef[row : row + 1, :] + coef[2 + row : 3 + row, :]
            hidden[r, :] = y.astype(BF16)
            return carry

        lax.fori_loop(0, rows // block, body, 0, unroll=min(4, rows // block))

    modulate(lambda r: context[r, :], ctx_rows, 1)
    raw = jnp.dot(hidden[0:ctx_rows, :], w_all[:, q_width:], preferred_element_type=F32)
    if groups == 2:
        k, val = raw[:, :kv_width], raw[:, kv_width:]
        lane = lax.broadcasted_iota(jnp.int32, k.shape, 1)
        first = lane < SPAN
        sq = k * k
        s0 = jnp.sum(jnp.where(first, sq, 0.0), axis=-1, keepdims=True)
        s1 = jnp.sum(jnp.where(first, 0.0, sq), axis=-1, keepdims=True)
        scale = jnp.where(
            first, lax.rsqrt(s0 / SPAN + epsilon), lax.rsqrt(s1 / SPAN + epsilon)
        )
        k = k * scale * k_pair
        ctx_send[0] = jnp.where(first, k, pltpu.roll(val, SPAN, 1)).astype(BF16)
        ctx_send[1] = jnp.where(first, pltpu.roll(k, SPAN, 1), val).astype(BF16)
    else:
        lane = lax.broadcasted_iota(jnp.int32, raw.shape, 1)
        first = lane < SPAN
        s0 = jnp.sum(jnp.where(first, raw * raw, 0.0), axis=-1, keepdims=True)
        k = raw * lax.rsqrt(s0 / SPAN + epsilon) * k_pair
        ctx_send[0] = jnp.where(first, k, raw).astype(BF16)
    far = [d for d in range(2, highs)] if highs > 2 else []
    z_order = far[:1] + [1] + far[1:] if highs > 1 else []
    tail_sends = []

    def ctx_copy(head, src, ssem, z, y):
        return remote(ctx_send.at[head], ctx_all.at[src], ssem, c_recv.at[src], (dev(z, y), tp))

    def finish(raw_head, gain, d):
        inv = lax.rsqrt(jnp.sum(raw_head * raw_head, axis=0, keepdims=True) / SPAN + epsilon)
        y = raw_head * inv * gain[...]
        a1, b1 = y[0:QUARTER], y[QUARTER : 2 * QUARTER]
        a2, b2 = y[2 * QUARTER : 3 * QUARTER], y[3 * QUARTER :]
        cr, sr = table[d, 0:QUARTER, :], table[d, QUARTER : 2 * QUARTER, :]
        cc, sc = table[d, 2 * QUARTER : 3 * QUARTER, :], table[d, 3 * QUARTER :, :]
        return jnp.concatenate(
            [a1 * cr - b1 * sr, b1 * cr + a1 * sr, a2 * cc - b2 * sc, b2 * cc + a2 * sc], axis=0
        )

    def q_copy(d, group, ssem, z):
        return remote(
            q_send.at[d, group], q_all.at[d * groups + g, :, 0:SPAN, :], ssem,
            q_rsem.at[d, g], (dev(z, low), tp),
        )

    def q_arrive(d, r):
        other = lax.rem(g + r, groups)
        remote(
            q_send.at[d, other], q_all.at[d * groups + other, :, 0:SPAN, :], q_ssem.at[d, 0],
            q_rsem.at[d, other], (dev(base + other, low), tp),
        ).wait_recv()

    def kv_copy(src_ref, d, src, ssem, z, y):
        return remote(
            src_ref, kv_all.at[d * n_sp + src], ssem, kv_recv.at[d, src], (dev(z, y), tp)
        )

    def project(d):
        chip = lax.rem(x - d + chips, chips)
        modulate(lambda r: lat[chip, r, :], width, 0)
        flat = jnp.dot(hidden[...], w_all[...], preferred_element_type=F32)
        up = jnp.transpose(flat)
        for j in range(groups):
            for h in range(heads):
                r = (j * heads + h) * SPAN
                y = finish(up[r : r + SPAN], gain_q, d)
                q_send[d, j, h] = (y * SPAN ** (-0.5)).astype(BF16)
            r = q_width + j * SPAN
            kv_send[d, j, 0:SPAN, :] = finish(up[r : r + SPAN], gain_k, d).astype(BF16)
            r = q_width + kv_width + j * SPAN
            kv_send[d, j, SPAN:, :] = up[r : r + SPAN].astype(BF16)
        for r in range(1, groups):
            other = lax.rem(g + r, groups)
            c = q_copy(d, other, q_ssem.at[d, r - 1], base + other)
            c.start()
            tail_sends.append(c)
        for n, dz in enumerate(z_order):
            z = lax.rem(high + dz, highs)
            head = lax.rem(z, groups)
            if d == 0:
                c = ctx_copy(head, sp, cz_send.at[dz - 1], z, low)
                c.start()
                tail_sends.append(c)
            c = kv_copy(kv_send.at[d, head], d, sp, z_send.at[d, dz - 1], z, low)
            c.start()
            tail_sends.append(c)
        for dl in range(1, lows):
            y = lax.rem(low + dl, lows)
            if d == 0:
                c = ctx_copy(g, sp, cy_send.at[dl - 1], high, y)
                c.start()
                tail_sends.append(c)
            c = kv_copy(kv_send.at[d, g], d, sp, y_send.at[d, dl - 1], high, y)
            c.start()
            tail_sends.append(c)
        q_all[d * groups + g, :, 0:SPAN, :] = q_send[d, g]
        kv_all[d * n_sp + sp] = kv_send[d, g]
        k_nat[d * n_sp + sp] = jnp.transpose(kv_send[d, g])
        if d == 0:
            ctx_all[sp] = ctx_send[g]

    def column(d, dz):
        src = dev(lax.rem(high - dz + highs, highs), low)
        slot = d * n_sp + src
        kv_copy(kv_all.at[slot], d, src, z_send.at[0, 0], high, low).wait_recv()
        for dl in range(1, lows):
            y = lax.rem(low + dl, lows)
            c = kv_copy(kv_all.at[slot], d, src, f_send.at[d, dz - 1, dl - 1], high, y)
            c.start()
            tail_sends.append(c)
        k_nat[slot] = jnp.transpose(kv_all[slot])
        if d == 0:
            ctx_copy(0, src, cz_send.at[0], high, low).wait_recv()
            for dl in range(1, lows):
                y = lax.rem(low + dl, lows)
                c = remote(
                    ctx_all.at[src], ctx_all.at[src], cf_send.at[dz - 1, dl - 1],
                    c_recv.at[src], (dev(high, y), tp),
                )
                c.start()
                tail_sends.append(c)

    def side(d, dz, dl):
        src = dev(lax.rem(high - dz + highs, highs), lax.rem(low - dl + lows, lows))
        slot = d * n_sp + src
        kv_copy(kv_all.at[slot], d, src, z_send.at[0, 0], high, low).wait_recv()
        k_nat[slot] = jnp.transpose(kv_all[slot])
        return slot

    def own_slot(d, dz):
        return d * n_sp + dev(lax.rem(high - dz + highs, highs), low)

    def attend(items):
        items = [(s, t, h, b) for s, t, b in items for h in range(heads)]
        n = len(items)
        scores = {}

        def score(i):
            s, t, h, b = items[i]
            r = jnp.dot(k_nat[s], q_all[t, h], preferred_element_type=F32)
            scores[i] = r + b if b else r

        for i in range(min(LAG, n)):
            score(i)
        for i in range(n):
            if i + LAG < n:
                score(i + LAG)
            slot, t, h, _ = items[i]
            s = scores.pop(i)
            old = peak[t, h, 0:1, :]
            top = jnp.maximum(jnp.max(s, axis=0, keepdims=True), old)
            shrink = jnp.exp2((old - top) * LOG2E)
            e = jnp.exp2((s - top) * LOG2E)
            total[t, h] = total[t, h] * shrink + jnp.sum(
                e.reshape(width // 8, 8, width), axis=0
            )
            peak[t, h] = jnp.broadcast_to(top, (8, width))
            w = jnp.dot(kv_all[slot, SPAN:, :], e.astype(BF16), preferred_element_type=F32)
            acc[t, h] = acc[t, h] * shrink + w

    def tiles(d):
        return range(d * groups, (d + 1) * groups)

    def attend_range(first, count, tile_list, shift):
        per = max(1, 8 // len(tile_list))
        per = math.gcd(per, count)

        def body(i, carry):
            attend(
                [(first + i * per + u, t, shift) for u in range(per) for t in tile_list]
            )
            return carry

        if count == per:
            body(0, 0)
        else:
            lax.fori_loop(0, count // per, body, 0)

    def fetch(d):
        chip = lax.rem(x - d + chips, chips)
        near, back = 2 * chip + core, 2 * chip + 1 - core
        for piece in range(PIECES):
            row_copy(near, piece, lat_send.at[0, 0], twin).wait_recv()
            c = row_copy(near, piece, lat_fwd.at[d - 1, piece], twin)
            c.start()
            tail_sends.append(c)
        return back

    def fetch_rest(back):
        for piece in range(PIECES):
            row_copy(back, piece, lat_send.at[0, 0], twin).wait_recv()

    project(0)
    pending = list(z_order)
    for d in range(chips):
        mine = [t for t in tiles(d)]
        so_far = [t for t in range((d + 1) * groups)]
        done = []
        for r in range(1, groups):
            q_arrive(d, r)
        if d > 0:
            segments = [(k * n_sp, n_sp) for k in range(d)]
            if len(segments) < len(pending):
                segments = [(k * n_sp // 2, n_sp // 2) for k in range(2 * d)]
            for first, count in segments:
                attend_range(first, count, mine, 0.0)
                if pending:
                    dz = pending.pop(0)
                    column(d, dz)
                    done.append(dz)
        if d == chips - 1:
            for dz in pending:
                column(d, dz)
                done.append(dz)
            pending = []
        else:
            attend([(own_slot(d, 0), t, 0.0) for t in so_far])
            dz = pending.pop(0)
            column(d, dz)
            attend([(own_slot(d, dz), t, 0.0) for t in so_far])
            back = fetch(d + 1)
            if pending:
                extra = pending.pop(0)
                column(d, extra)
                done.append(extra)
            fetch_rest(back)
            project(d + 1)
            for dz in pending:
                column(d, dz)
                done.append(dz)
            pending = list(z_order)
        if d == chips - 1:
            done = [0] + done
        if d == 0:
            for dl in range(1, lows):
                for dz in range(highs):
                    src = dev(
                        lax.rem(high - dz + highs, highs), lax.rem(low - dl + lows, lows)
                    )
                    ctx_copy(0, src, cz_send.at[0], high, low).wait_recv()
            for c in range(ctx_slots):
                per = width // ctx_rows
                piece = ctx_all[c * per : (c + 1) * per].reshape(width, 2 * SPAN)
                k_nat[ctx_first + c] = piece
                kv_all[ctx_first + c] = jnp.transpose(piece)
        for i in range(0, len(done), 2):
            attend([(own_slot(d, dz), t, 0.0) for dz in done[i : i + 2] for t in so_far])
        attend_range(ctx_first, ctx_slots, mine, offset)
        for dl in range(1, lows):
            order = [0] + list(z_order)
            for i in range(0, len(order), 2):
                slots = [side(d, dz, dl) for dz in order[i : i + 2]]
                attend([(s, t, 0.0) for s in slots for t in so_far])

    copies = []
    for d in range(chips):
        chip = lax.rem(x - d + chips, chips)
        for r in reversed(range(groups)):
            j = lax.rem(g + r, groups)
            t = d * groups + j
            rows = []
            for h in range(heads):
                inv = 1.0 / jnp.sum(total[t, h], axis=0, keepdims=True)
                rows.append(acc[t, h] * inv)
            attended[d, r] = jnp.transpose(jnp.concatenate(rows, axis=0)).astype(BF16)
            for rc in range(2):
                half = lax.rem(core + rc, 2)
                src = attended.at[
                    d, r, pl.ds(pl.multiple_of(half * own_rows, own_rows), own_rows), :
                ]
                if d == 0 and r == 0 and rc == 0:
                    received[tp * groups + g] = src[...]
                else:
                    c = remote(
                        src, received.at[tp * groups + g], at_send.at[d, r, rc],
                        at_recv.at[tp * groups + g],
                        (dev(base + j, low), 2 * chip + half),
                    )
                    c.start()
                    copies.append(c)
    loads[-1].wait()
    for rt in range(n_tp):
        for r in range(groups):
            if rt == 0 and r == 0:
                continue
            who = lax.rem(tp + rt, n_tp) * groups + lax.rem(g + r, groups)
            remote(
                received.at[who], received.at[who], at_send.at[0, 0, 1], at_recv.at[who],
                (sp, twin),
            ).wait_recv()
    rows = jnp.concatenate([received[s] for s in range(n_tp * groups)], axis=1)
    own = pl.ds(pl.multiple_of(core * own_rows, own_rows), own_rows)
    for t in range(n_tp):
        cols = slice(t * columns, (t + 1) * columns)
        branch = jnp.dot(rows, w_out[:, cols], preferred_element_type=F32)
        out[:, cols] = (lat[x, own, cols].astype(F32) + mods[t, 4:5, :] * branch).astype(BF16)
    for c in lat_sends + tail_sends + copies:
        c.wait_send()


def on_device(
    latent, context, condition, context_condition, norm_gain, shift_weight, scale_weight,
    gate_weight, query_weight, key_weight, value_weight, query_gain, key_gain, output_weight,
):
    n_sp, n_tp = lax.axis_size("sp"), lax.axis_size("tp")
    row_slab, columns = shift_weight.shape
    own_rows, model = latent.shape
    ctx_rows = context.shape[0]
    tok = own_rows * n_tp
    q_width, kv_width = query_weight.shape[1], key_weight.shape[1]
    groups = kv_width // SPAN
    heads = q_width // SPAN // groups
    chips = n_tp // 2
    width = 2 * own_rows
    lows = 2 ** (int(math.log2(n_sp)) // 2)
    highs = n_sp // lows
    slots = chips * n_sp + n_sp * ctx_rows // width
    n_tiles = chips * groups
    offset = math.log(tok / (2.0 * ctx_rows))
    dma = pltpu.SemaphoreType.DMA
    return pl.pallas_call(
        functools.partial(kernel, n_sp, n_tp, lows, offset),
        out_shape=jax.ShapeDtypeStruct(latent.shape, BF16),
        in_specs=[ANY] * 2 + [VMEM] * 3 + [ANY] * 6 + [VMEM] * 2 + [ANY],
        out_specs=VMEM,
        scratch_shapes=[
            pltpu.VMEM((chips, width, model), BF16),
            pltpu.VMEM(context.shape, BF16),
            pltpu.VMEM((3, row_slab, columns), BF16),
            pltpu.VMEM((model, q_width + 2 * kv_width), BF16),
            pltpu.VMEM((2,) + (key_weight.shape if kv_width % 128 else (16, 128)), BF16),
            pltpu.VMEM(output_weight.shape, BF16),
            pltpu.VMEM((8, columns), F32),
            pltpu.VMEM((n_sp, 8, columns), F32),
            pltpu.VMEM((n_tp, 8, columns), F32),
            pltpu.VMEM((8, model), F32),
            pltpu.VMEM((width, model), BF16),
            pltpu.VMEM((chips, SPAN, width), F32),
            pltpu.VMEM((SPAN, width), F32),
            pltpu.VMEM((SPAN, width), F32),
            pltpu.VMEM((chips, groups, heads, SPAN, width), BF16),
            pltpu.VMEM((chips, groups, 2 * SPAN, width), BF16),
            pltpu.VMEM((groups, ctx_rows, 2 * SPAN), BF16),
            pltpu.VMEM((n_sp, ctx_rows, 2 * SPAN), BF16),
            pltpu.VMEM((n_tiles, heads, 2 * SPAN, width), BF16),
            pltpu.VMEM((slots, 2 * SPAN, width), BF16),
            pltpu.VMEM((slots, width, 2 * SPAN), BF16),
            pltpu.VMEM((n_tiles, heads, 8, width), F32),
            pltpu.VMEM((n_tiles, heads, 8, width), F32),
            pltpu.VMEM((n_tiles, heads, SPAN, width), F32),
            pltpu.VMEM((chips, groups, width, 2 * SPAN), BF16),
            pltpu.VMEM((n_tp * groups, own_rows, 2 * SPAN), BF16),
            dma((9,)), dma((chips, PIECES)), dma((max(chips - 1, 1), PIECES)), dma((n_tp, PIECES)),
            dma((n_sp - 1,)), dma((n_sp - 1,)), dma((n_tp - 1,)), dma((n_tp - 1,)),
            dma((chips, max(groups - 1, 1))), dma((chips, groups)),
            dma((chips, highs - 1)), dma((chips, lows - 1)),
            dma((chips, highs - 1, lows - 1)), dma((chips, n_sp)),
            dma((highs - 1,)), dma((lows - 1,)), dma((highs - 1, lows - 1)), dma((n_sp,)),
            dma((chips, groups, 2)), dma((n_tp * groups,)),
        ],
        compiler_params=pltpu.CompilerParams(
            collective_id=0, has_side_effects=True, vmem_limit_bytes=60 << 20
        ),
        name="fused",
    )(
        latent, context, condition[None], context_condition[None], norm_gain[None],
        shift_weight, scale_weight, gate_weight, query_weight, key_weight, value_weight,
        query_gain[None], key_gain[None], output_weight,
    )


def solution(mesh):
    in_specs = (
        P(("sp", "tp"), None), P("sp", None), P(), P(), P(),
        P("sp", "tp"), P("sp", "tp"), P("sp", "tp"),
        P(None, "tp"), P(None, "tp"), P(None, "tp"), P(), P(), P(),
    )
    return jax.shard_map(
        on_device, mesh=mesh, in_specs=in_specs, out_specs=P(("sp", "tp"), None), check_vma=False
    )
```

time: 82.1 us -> 59.3 us (0.72)
  the two profiles are of different devices: /device:TPU:25 before, /device:TPU:0 now
where the time goes in v1:
time: 59.3 us; the launch traced here: 59.1 us
  Pallas kernels  57.2 us (96%)
  local copies, waits for them, and re-layouts  1.88 us (3%)
    pallas_call x1, Pallas kernels, on_device(): pl.pallas_call(functools.partial(kernel, n_sp, n_tp, lows, offset), out_s...  57.2 us
    unnamed x1, local copies, waits for them, and re-layouts  1.88 us

profile of v1, /device:TPU:0, one launch (start us, length us, event | category | flops | bytes accessed | tf_op | source)
XLA Modules:
  0.0 59.1 jit_solution(6482469846581508600)
XLA Ops:
  0.0 57.2 %fused.1 = bf16[128,2048]{1,0:T(8,128)(2,1)} custom-call(bf16[128,2048]{1,0:T(8,128)(2,1)} %latent_hbm.1, bf16[64,2048]{1,0:T(8,128)(2,1)} %context_hbm.1, f32[1,2048]{1,0:T(1,128)} %bitcast.5, f32[1,2048]{1,0:T(1,128)} %bitcast.6, f32[1,2048]{1,0:T(1,128)} %bitcast.7, bf16[256,512]{1,0:T(8,128)(2,1)} %w_shift_hbm.1, bf16[256,512]{1,0:T(8,128)(2,1)} %w_scale_hbm.1, ...), custom_call_target="tpu_custom_call" | custom-call | tf_op jit(solution)/shard_map/fused/pallas_call | solution.py:537
  57.2 1.9 %copy.16 = bf16[128,2048]{1,0:T(8,128)(2,1)} copy(bf16[128,2048]{1,0:T(8,128)(2,1)} %fused.1) | data formatting | bytes 1048576

commit v2 on v1

v2 whole, which is shorter than its diff:
```python
import functools
import math

import jax
import jax.numpy as jnp
from jax import lax
from jax.experimental import pallas as pl
from jax.experimental.pallas import tpu as pltpu
from jax.sharding import PartitionSpec as P

SPAN = 64
GRID_W = 64
QUARTER = SPAN // 4
LAG = 6
PIECES = 2
LOG2E = 1.4426950408889634
MESH = pl.DeviceIdType.MESH
VMEM = pl.BlockSpec(memory_space=pltpu.VMEM)
ANY = pl.BlockSpec(memory_space=pl.ANY)
F32 = jnp.float32
BF16 = jnp.bfloat16

epsilon = 1e-06
rope_base = 10000.0


def kernel(
    n_sp, n_tp, lows, offset, split,
    latent_hbm, context_hbm, cond, ctx_cond, norm_gain, w_shift_hbm, w_scale_hbm, w_gate_hbm,
    w_q_hbm, w_k_hbm, w_v_hbm, q_gain, k_gain, w_out_hbm,
    out,
    lat, context, w_mod, w_all, w_side, w_out, part, parts, mods, part_g, parts_g, mods_g,
    coef, hidden, table, gain_q, gain_k, q_send, q_raw, kv_send, ctx_send, ctx_all, q_all, kv_all,
    k_nat, peak, acc, attended, received,
    load, lat_send, lat_fwd, lat_recv, sp_send, sp_recv, tp_send, tp_recv,
    q_ssem, q_rsem, z_send, y_send, f_send, kv_recv,
    cz_send, cy_send, cf_send, c_recv, at_send, at_recv,
):
    sp, tp = lax.axis_index("sp"), lax.axis_index("tp")
    chips = n_tp // 2
    highs = n_sp // lows
    low, high = lax.rem(sp, lows), sp // lows
    x, core = tp // 2, lax.rem(tp, 2)
    twin = tp + 1 - 2 * core
    width = lat.shape[1]
    own_rows = width // 2
    model = lat.shape[2]
    tok = chips * width
    ctx_rows = context.shape[0]
    groups = kv_send.shape[1]
    heads = q_send.shape[2]
    q_width = groups * heads * SPAN
    kv_width = groups * SPAN
    row_slab, columns = w_mod.shape[1], w_mod.shape[2]
    bands = columns // 128
    g = lax.rem(high, groups)
    base = high - g
    ctx_slots = n_sp * ctx_rows // width
    ctx_first = chips * n_sp
    step = own_rows // PIECES
    part_width = width // split

    def dev(z, y):
        return z * lows + y

    def remote(src, dst, ssem, rsem, peer):
        return pltpu.make_async_remote_copy(
            src_ref=src, dst_ref=dst, send_sem=ssem, recv_sem=rsem,
            device_id=peer, device_id_type=MESH,
        )

    def lanes_of(d, p):
        if d == 0 or split == 1:
            return slice(0, width)
        return slice(p * part_width, (p + 1) * part_width)

    def parts_in(d):
        return 1 if d == 0 else split

    barrier = pltpu.get_barrier_semaphore()
    peers = [(lax.rem(sp + d, n_sp), tp) for d in range(1, n_sp)]
    peers += [(sp, lax.rem(tp + d, n_tp)) for d in range(1, n_tp)]
    for r in range(1, groups):
        mate = dev(base + lax.rem(g + r, groups), low)
        peers += [(mate, lax.rem(tp + d, n_tp)) for d in range(1, n_tp)]
    for p in peers:
        pl.semaphore_signal(barrier, inc=1, device_id=p, device_id_type=MESH)

    mine_rows = pl.ds(pl.multiple_of(core * own_rows, own_rows), own_rows)
    pairs = [
        (w_shift_hbm, w_mod.at[0]), (w_scale_hbm, w_mod.at[1]),
        (latent_hbm, lat.at[x, mine_rows, :]), (w_gate_hbm, w_mod.at[2]),
        (context_hbm, context), (w_q_hbm, w_all.at[:, 0:q_width]),
    ]
    if kv_width % 128 == 0:
        pairs += [
            (w_k_hbm, w_all.at[:, q_width : q_width + kv_width]),
            (w_v_hbm, w_all.at[:, q_width + kv_width :]),
        ]
    else:
        pairs += [(w_k_hbm, w_side.at[0]), (w_v_hbm, w_side.at[1])]
    pairs.append((w_out_hbm, w_out))
    loads = [pltpu.make_async_copy(s, d, load.at[i]) for i, (s, d) in enumerate(pairs)]
    for c in loads[:-1]:
        c.start()

    def slab(ref):
        if row_slab % 128 == 0:
            return ref[:, pl.ds(pl.multiple_of(sp * row_slab, 128), row_slab)]
        per = 128 // row_slab
        window = ref[:, pl.ds(pl.multiple_of(sp // per * 128, 128), 128)]
        pick = lax.rem(sp, per)
        result = window
        for k in range(1, per):
            result = jnp.where(pick == k, pltpu.roll(window, 128 - k * row_slab, 1), result)
        return result[:, :row_slab]

    v = jnp.concatenate([slab(cond), slab(ctx_cond)], axis=0)
    act = (v / (1.0 + jnp.exp(-v))).astype(BF16)
    part_g[...] = jnp.zeros_like(part_g)
    for i in range(2):
        loads[i].wait()
        r = jnp.dot(act, w_mod[i], preferred_element_type=F32)
        for row in range(2):
            for k in range(bands):
                at = (2 * i + row) * bands + k
                part[at : at + 1, :] = r[row : row + 1, k * 128 : (k + 1) * 128]
    loads[2].wait()
    pl.semaphore_wait(barrier, len(peers))

    def rows_of(tile, piece):
        chip, half = tile // 2, lax.rem(tile, 2)
        start = pl.multiple_of(half * own_rows + piece * step, step)
        return lat.at[chip, pl.ds(start, step), :]

    def row_copy(tile, piece, ssem, peer):
        return remote(
            rows_of(tile, piece), rows_of(tile, piece), ssem, lat_recv.at[tile, piece], (sp, peer)
        )

    lat_sends = []

    def send_piece(piece):
        for d in range(1, chips):
            c = row_copy(tp, piece, lat_send.at[d, piece], lax.rem(tp + 2 * d, n_tp))
            c.start()
            lat_sends.append(c)

    sp_copies = []
    for d in range(1, n_sp):
        c = remote(
            part, parts.at[sp], sp_send.at[0, d - 1], sp_recv.at[0, d - 1],
            (lax.rem(sp + d, n_sp), tp),
        )
        c.start()
        sp_copies.append(c)
    send_piece(0)
    for piece in range(PIECES):
        c = row_copy(tp, piece, lat_send.at[0, piece], twin)
        c.start()
        lat_sends.append(c)
    parts[sp] = part[...]

    loads[3].wait()
    r = jnp.dot(act, w_mod[2], preferred_element_type=F32)
    for k in range(bands):
        part_g[k : k + 1, :] = r[0:1, k * 128 : (k + 1) * 128]
    parts_g[sp] = part_g[...]
    loads[-1].start()
    for d in range(chips):
        chip = lax.rem(x - d + chips, chips)
        lane = lax.broadcasted_iota(jnp.int32, (QUARTER, width), 1)
        if parts_in(d) > 1:
            lane = lane // step % 2 * own_rows + lane // part_width * step + lane % step
        place = sp * tok + chip * width + lane
        turn = lax.broadcasted_iota(jnp.int32, (QUARTER, width), 0).astype(F32)
        freq = jnp.exp(turn * (-math.log(rope_base) / QUARTER))
        by_row = (place // GRID_W).astype(F32) * freq
        by_col = (place % GRID_W).astype(F32) * freq
        table[d, 0:QUARTER, :] = jnp.cos(by_row)
        table[d, QUARTER : 2 * QUARTER, :] = jnp.sin(by_row)
        table[d, 2 * QUARTER : 3 * QUARTER, :] = jnp.cos(by_col)
        table[d, 3 * QUARTER :, :] = jnp.sin(by_col)
    k_pair = jnp.concatenate([k_gain[...], k_gain[...]], axis=1)
    for ref, dst in ((q_gain, gain_q), (k_gain, gain_k)):
        row = jnp.concatenate([ref[...], ref[...]], axis=1)
        square = jnp.transpose(jnp.broadcast_to(row, (128, 128)))[0:SPAN, :]
        for c in range(0, width, 128):
            dst[:, c : c + 128] = square
    peak[...] = jnp.full_like(peak, -1e30)
    acc[...] = jnp.zeros_like(acc)
    kv_all[:, 2 * SPAN :, :] = jnp.ones((kv_all.shape[0], 16, width), BF16)

    for c in sp_copies:
        c.wait()
    summed = parts[0]
    for j in range(1, n_sp):
        summed = summed + parts[j]
    part[...] = summed
    mods[tp] = summed
    tp_copies = []
    for d in range(1, n_tp):
        c = remote(
            part, mods.at[tp], tp_send.at[0, d - 1], tp_recv.at[0, d - 1],
            (sp, lax.rem(tp + d, n_tp)),
        )
        c.start()
        tp_copies.append(c)
    for piece in range(1, PIECES):
        send_piece(piece)
    gate_copies = []
    for d in range(1, n_sp):
        c = remote(
            part_g, parts_g.at[sp], sp_send.at[1, d - 1], sp_recv.at[1, d - 1],
            (lax.rem(sp + d, n_sp), tp),
        )
        c.start()
        gate_copies.append(c)
    for c in loads[4:-1]:
        c.wait()
    if kv_width % 128 != 0:
        w_all[:, q_width:] = jnp.concatenate([w_side[0], w_side[1]], axis=1)
    for piece in range(PIECES):
        row_copy(twin, piece, lat_send.at[0, 0], twin).wait_recv()
    for c in tp_copies:
        c.wait()
    for t in range(n_tp):
        for k in range(bands):
            cols = slice(t * columns + k * 128, t * columns + (k + 1) * 128)
            for row in range(2):
                at = (2 + row) * bands + k
                coef[row : row + 1, cols] = norm_gain[:, cols] * (1.0 + mods[t, at : at + 1, :])
                at = row * bands + k
                coef[2 + row : 3 + row, cols] = mods[t, at : at + 1, :]

    block = 16

    def modulate(read, rows, first, row):
        def body(i, carry):
            w = read(i * block).astype(F32)
            inv = lax.rsqrt(jnp.sum(w * w, axis=-1, keepdims=True) / model + epsilon)
            y = w * inv * coef[row : row + 1, :] + coef[2 + row : 3 + row, :]
            hidden[pl.ds(pl.multiple_of(first + i * block, block), block), :] = y.astype(BF16)
            return carry

        lax.fori_loop(0, rows // block, body, 0, unroll=min(4, rows // block))

    far = [d for d in range(2, highs)] if highs > 2 else []
    z_order = far[:1] + [1] + far[1:] if highs > 1 else []
    tail_sends = []

    def begin(c):
        c.start()
        tail_sends.append(c)

    def ctx_copy(head, src, ssem, z, y):
        return remote(ctx_send.at[head], ctx_all.at[src], ssem, c_recv.at[src], (dev(z, y), tp))

    def context_step():
        modulate(
            lambda i: context[pl.ds(pl.multiple_of(i, block), block), :], ctx_rows, 0, 1
        )
        raw = jnp.dot(hidden[0:ctx_rows, :], w_all[:, q_width:], preferred_element_type=F32)
        if groups == 2:
            k, val = raw[:, :kv_width], raw[:, kv_width:]
            first = lax.broadcasted_iota(jnp.int32, k.shape, 1) < SPAN
            sq = k * k
            s0 = jnp.sum(jnp.where(first, sq, 0.0), axis=-1, keepdims=True)
            s1 = jnp.sum(jnp.where(first, 0.0, sq), axis=-1, keepdims=True)
            scale = jnp.where(
                first, lax.rsqrt(s0 / SPAN + epsilon), lax.rsqrt(s1 / SPAN + epsilon)
            )
            k = k * scale * k_pair
            ctx_send[0] = jnp.where(first, k, pltpu.roll(val, SPAN, 1)).astype(BF16)
            ctx_send[1] = jnp.where(first, pltpu.roll(k, SPAN, 1), val).astype(BF16)
        else:
            first = lax.broadcasted_iota(jnp.int32, raw.shape, 1) < SPAN
            s0 = jnp.sum(jnp.where(first, raw * raw, 0.0), axis=-1, keepdims=True)
            k = raw * lax.rsqrt(s0 / SPAN + epsilon) * k_pair
            ctx_send[0] = jnp.where(first, k, raw).astype(BF16)
        for dz in z_order:
            z = lax.rem(high + dz, highs)
            begin(ctx_copy(lax.rem(z, groups), sp, cz_send.at[dz - 1], z, low))
        for dl in range(1, lows):
            begin(ctx_copy(g, sp, cy_send.at[dl - 1], high, lax.rem(low + dl, lows)))
        ctx_all[sp] = ctx_send[g]

    def finish(raw_head, gain, d, lanes):
        n = lanes.stop - lanes.start
        inv = lax.rsqrt(jnp.sum(raw_head * raw_head, axis=0, keepdims=True) / SPAN + epsilon)
        y = raw_head * inv * gain[:, 0:n]
        a1, b1 = y[0:QUARTER], y[QUARTER : 2 * QUARTER]
        a2, b2 = y[2 * QUARTER : 3 * QUARTER], y[3 * QUARTER :]
        cr, sr = table[d, 0:QUARTER, lanes], table[d, QUARTER : 2 * QUARTER, lanes]
        cc, sc = table[d, 2 * QUARTER : 3 * QUARTER, lanes], table[d, 3 * QUARTER :, lanes]
        return jnp.concatenate(
            [a1 * cr - b1 * sr, b1 * cr + a1 * sr, a2 * cc - b2 * sc, b2 * cc + a2 * sc], axis=0
        )

    def q_copy(d, p, group, ssem, z):
        lanes = lanes_of(d, p)
        return remote(
            q_send.at[d, group, :, :, lanes], q_raw.at[d, g, :, :, lanes], ssem,
            q_rsem.at[d, p, g], (dev(z, low), tp),
        )

    def q_store(d, group, value):
        f = value.astype(F32) * LOG2E
        hi = f.astype(BF16)
        q_all[d * groups + group, :, 0:SPAN, :] = hi
        q_all[d * groups + group, :, SPAN:, :] = (f - hi.astype(F32)).astype(BF16)

    def q_own(d):
        q_store(d, g, q_send[d, g])

    def q_arrive(d):
        for r in range(1, groups):
            other = lax.rem(g + r, groups)
            for p in range(parts_in(d)):
                lanes = lanes_of(d, p)
                dst = q_raw.at[d, other, :, :, lanes]
                remote(
                    dst, dst, q_ssem.at[d, 0, 0], q_rsem.at[d, p, other], (dev(base + other, low), tp)
                ).wait_recv()
            q_store(d, other, q_raw[d, other])

    def kv_copy(src_ref, d, p, src, ssem, z, y):
        lanes = lanes_of(d, p)
        return remote(
            src_ref, kv_all.at[d * n_sp + src, 0 : 2 * SPAN, lanes], ssem, kv_recv.at[d, p, src],
            (dev(z, y), tp),
        )

    def key_rows(slot, lanes):
        k = kv_all[slot, 0:SPAN, lanes]
        k_nat[slot, lanes, :] = jnp.transpose(jnp.concatenate([k, k], axis=0))

    def project(d, p):
        chip = lax.rem(x - d + chips, chips)
        lanes = lanes_of(d, p)
        n = lanes.stop - lanes.start
        if n == width:
            modulate(
                lambda i: lat[chip, pl.ds(pl.multiple_of(i, block), block), :], width, 0, 0
            )
        else:
            for half in range(2):
                at = half * own_rows + p * step
                modulate(
                    lambda i: lat[chip, pl.ds(pl.multiple_of(at + i, block), block), :],
                    step, half * step, 0,
                )
        flat = jnp.dot(hidden[0:n, :], w_all[...], preferred_element_type=F32)
        up = jnp.transpose(flat)
        for j in range(groups):
            r = q_width + j * SPAN
            kv_send[d, j, 0:SPAN, lanes] = finish(up[r : r + SPAN], gain_k, d, lanes).astype(BF16)
            r = q_width + kv_width + j * SPAN
            kv_send[d, j, SPAN:, lanes] = up[r : r + SPAN].astype(BF16)
            for h in range(heads):
                r = (j * heads + h) * SPAN
                y = finish(up[r : r + SPAN], gain_q, d, lanes)
                q_send[d, j, h, :, lanes] = (y * SPAN ** (-0.5)).astype(BF16)
        for r in range(1, groups):
            other = lax.rem(g + r, groups)
            begin(q_copy(d, p, other, q_ssem.at[d, p, r - 1], base + other))
        for dz in z_order:
            z = lax.rem(high + dz, highs)
            src = kv_send.at[d, lax.rem(z, groups), :, lanes]
            begin(kv_copy(src, d, p, sp, z_send.at[d, p, dz - 1], z, low))
        for dl in range(1, lows):
            y = lax.rem(low + dl, lows)
            src = kv_send.at[d, g, :, lanes]
            begin(kv_copy(src, d, p, sp, y_send.at[d, p, dl - 1], high, y))
        kv_all[d * n_sp + sp, 0 : 2 * SPAN, lanes] = kv_send[d, g, :, lanes]
        key_rows(d * n_sp + sp, lanes)

    def column(d, p, dz):
        src = dev(lax.rem(high - dz + highs, highs), low)
        slot = d * n_sp + src
        lanes = lanes_of(d, p)
        here = kv_all.at[slot, 0 : 2 * SPAN, lanes]
        kv_copy(here, d, p, src, z_send.at[0, 0, 0], high, low).wait_recv()
        for dl in range(1, lows):
            y = lax.rem(low + dl, lows)
            begin(kv_copy(here, d, p, src, f_send.at[d, p, dz - 1, dl - 1], high, y))
        key_rows(slot, lanes)

    def ctx_column(dz):
        src = dev(lax.rem(high - dz + highs, highs), low)
        ctx_copy(0, src, cz_send.at[0], high, low).wait_recv()
        for dl in range(1, lows):
            y = lax.rem(low + dl, lows)
            begin(
                remote(
                    ctx_all.at[src], ctx_all.at[src], cf_send.at[dz - 1, dl - 1],
                    c_recv.at[src], (dev(high, y), tp),
                )
            )

    def side(d, dz, dl):
        src = dev(lax.rem(high - dz + highs, highs), lax.rem(low - dl + lows, lows))
        slot = d * n_sp + src
        for p in range(parts_in(d)):
            lanes = lanes_of(d, p)
            here = kv_all.at[slot, 0 : 2 * SPAN, lanes]
            kv_copy(here, d, p, src, z_send.at[0, 0, 0], high, low).wait_recv()
            key_rows(slot, lanes)

    def ctx_ready():
        for dl in range(1, lows):
            for dz in range(highs):
                src = dev(lax.rem(high - dz + highs, highs), lax.rem(low - dl + lows, lows))
                ctx_copy(0, src, cz_send.at[0], high, low).wait_recv()
        per = width // ctx_rows
        for c in range(ctx_slots):
            piece = ctx_all[c * per : (c + 1) * per].reshape(width, 2 * SPAN)
            kv_all[ctx_first + c, 0 : 2 * SPAN, :] = jnp.transpose(piece)
            key_rows(ctx_first + c, slice(0, width))

    def slot_of(d, dz, dl):
        return d * n_sp + dev(
            lax.rem(high - dz + highs, highs), lax.rem(low - dl + lows, lows)
        )

    def attend(items):
        items = [(s, t, h) for s, t in items for h in range(heads)]
        n = len(items)
        scores = {}

        def score(i):
            s, t, h = items[i]
            r = jnp.dot(k_nat[s], q_all[t, h], preferred_element_type=F32)
            if isinstance(s, int) and s >= ctx_first:
                r = r + offset * LOG2E
            scores[i] = r

        for i in range(min(LAG, n)):
            score(i)
        for i in range(n):
            if i + LAG < n:
                score(i + LAG)
            slot, t, h = items[i]
            s = scores.pop(i)
            old = peak[t, h, 0:1, :]
            top = jnp.maximum(jnp.max(s, axis=0, keepdims=True), old)
            shrink = jnp.exp2(old - top)
            e = jnp.exp2(s - top).astype(BF16)
            peak[t, h] = jnp.broadcast_to(top, (8, width))
            w = jnp.dot(kv_all[slot, SPAN:, :], e, preferred_element_type=F32)
            acc[t, h] = acc[t, h] * shrink + w

    def attend_range(first, count, tile_list):
        per = math.gcd(max(1, 8 // len(tile_list)), count)

        def body(i, carry):
            attend([(first + i * per + u, t) for u in range(per) for t in tile_list])
            return carry

        lax.fori_loop(0, count // per, body, 0)

    def fetch(d, piece):
        chip = lax.rem(x - d + chips, chips)
        near = 2 * chip + core
        row_copy(near, piece, lat_send.at[0, 0], twin).wait_recv()
        begin(row_copy(near, piece, lat_fwd.at[d - 1, piece], twin))

    def fetch_back(d, piece):
        chip = lax.rem(x - d + chips, chips)
        row_copy(2 * chip + 1 - core, piece, lat_send.at[0, 0], twin).wait_recv()

    copies = []

    def deliver(d, r):
        chip = lax.rem(x - d + chips, chips)
        j = lax.rem(g + r, groups)
        t = d * groups + j
        rows = []
        for h in range(heads):
            inv = 1.0 / acc[t, h, SPAN : SPAN + 1, :]
            rows.append(acc[t, h, 0:SPAN, :] * inv)
        turned = jnp.transpose(jnp.concatenate(rows, axis=0)).astype(BF16)
        if parts_in(d) == 1:
            attended[d, r] = turned
        else:
            for p in range(split):
                for half in range(2):
                    at = half * own_rows + p * step
                    took = p * part_width + half * step
                    attended[d, r, at : at + step, :] = turned[took : took + step]
        for rc in range(2):
            half = lax.rem(core + rc, 2)
            src = attended.at[d, r, pl.ds(pl.multiple_of(half * own_rows, own_rows), own_rows), :]
            if d == 0 and r == 0 and rc == 0:
                received[tp * groups + g] = src[...]
            else:
                c = remote(
                    src, received.at[tp * groups + g], at_send.at[d, r, rc],
                    at_recv.at[tp * groups + g], (dev(base + j, low), 2 * chip + half),
                )
                c.start()
                copies.append(c)

    def gates():
        for c in gate_copies:
            c.wait()
        whole = parts_g[0]
        for j in range(1, n_sp):
            whole = whole + parts_g[j]
        part_g[...] = whole
        mods_g[tp] = whole
        result = []
        for d in range(1, n_tp):
            c = remote(
                part_g, mods_g.at[tp], tp_send.at[1, d - 1], tp_recv.at[1, d - 1],
                (sp, lax.rem(tp + d, n_tp)),
            )
            c.start()
            result.append(c)
        return result

    def tile_of(d, r):
        return d * groups + lax.rem(g + r, groups)

    if chips == 2 and split == 2 and n_sp == 8 and groups == 2:
        project(0, 0)
        fetch(1, 0)
        context_step()
        fetch_back(1, 0)
        project(1, 0)
        gate_out = gates()
        early = [tile_of(0, 0), tile_of(0, 1)]
        q_own(0)
        q_arrive(0)
        za, zb, zc = z_order
        attend([(slot_of(0, 0, 0), t) for t in early])
        column(0, 0, za)
        column(0, 0, zb)
        fetch(1, 1)
        attend([(slot_of(0, dz, 0), t) for dz in (za, zb) for t in early])
        column(0, 0, zc)
        for dz in z_order:
            ctx_column(dz)
        fetch_back(1, 1)
        project(1, 1)
        q_own(1)
        side(0, 0, 1)
        attend([(slot_of(0, zc, 0), t) for t in early] + [(slot_of(0, 0, 1), t) for t in early])
        column(1, 0, za)
        side(0, za, 1)
        side(0, zb, 1)
        attend([(slot_of(0, dz, 1), t) for dz in (za, zb) for t in early])
        column(1, 0, zb)
        column(1, 0, zc)
        ctx_ready()
        own_b, mate_b = tile_of(1, 0), tile_of(1, 1)
        ctx = range(ctx_first, ctx_first + ctx_slots)
        attend([(s, t) for s in ctx for t in early + [own_b]])
        column(1, 1, za)
        side(0, zc, 1)
        attend(
            [(slot_of(0, zc, 1), t) for t in early]
            + [(s, own_b) for s in range(0, n_sp // 2)]
        )
        column(1, 1, zb)
        attend([(s, own_b) for s in range(n_sp // 2, n_sp)])
        column(1, 1, zc)
        q_arrive(1)
        attend([(s, mate_b) for s in list(range(n_sp)) + list(ctx)])
        every = [tile_of(0, 1), mate_b, own_b, tile_of(0, 0)]
        attend([(slot_of(1, dz, 0), t) for dz in (0, za) for t in every])
        attend([(slot_of(1, dz, 0), t) for dz in (zb, zc) for t in every])
        last = [0] + z_order
        for dz in last:
            side(1, dz, 1)
        for (d, r), t in zip(((0, 1), (1, 1), (1, 0), (0, 0)), every):
            attend([(slot_of(1, dz, 1), t) for dz in last])
            deliver(d, r)
    else:
        context_step()
        for d in range(chips):
            if d > 0:
                for piece in range(PIECES):
                    fetch(d, piece)
                for piece in range(PIECES):
                    fetch_back(d, piece)
            for p in range(parts_in(d)):
                project(d, p)
            q_own(d)
        gate_out = gates()
        for dz in z_order:
            ctx_column(dz)
        for d in range(chips):
            for p in range(parts_in(d)):
                for dz in z_order:
                    column(d, p, dz)
            q_arrive(d)
        ctx_ready()
        for d in range(chips):
            for dl in range(1, lows):
                for dz in range(highs):
                    side(d, dz, dl)
        for d in range(chips):
            for r in range(groups):
                t = tile_of(d, r)
                attend_range(0, ctx_first, [t])
                attend([(s, t) for s in range(ctx_first, ctx_first + ctx_slots)])
                deliver(d, r)

    loads[-1].wait()
    for c in gate_out:
        c.wait()
    for rt in range(n_tp):
        for r in range(groups):
            if rt == 0 and r == 0:
                continue
            who = lax.rem(tp + rt, n_tp) * groups + lax.rem(g + r, groups)
            remote(
                received.at[who], received.at[who], at_send.at[0, 0, 1], at_recv.at[who],
                (sp, twin),
            ).wait_recv()
    rows = jnp.concatenate([received[s] for s in range(n_tp * groups)], axis=1)
    for t in range(n_tp):
        cols = slice(t * columns, (t + 1) * columns)
        gate = jnp.concatenate([mods_g[t, k : k + 1, :] for k in range(bands)], axis=1)
        branch = jnp.dot(rows, w_out[:, cols], preferred_element_type=F32)
        out[:, cols] = (lat[x, mine_rows, cols].astype(F32) + gate * branch).astype(BF16)
    for c in lat_sends + tail_sends + copies:
        c.wait_send()


def on_device(
    latent, context, condition, context_condition, norm_gain, shift_weight, scale_weight,
    gate_weight, query_weight, key_weight, value_weight, query_gain, key_gain, output_weight,
):
    n_sp, n_tp = lax.axis_size("sp"), lax.axis_size("tp")
    row_slab, columns = shift_weight.shape
    own_rows, model = latent.shape
    ctx_rows = context.shape[0]
    tok = own_rows * n_tp
    q_width, kv_width = query_weight.shape[1], key_weight.shape[1]
    groups = kv_width // SPAN
    heads = q_width // SPAN // groups
    chips = n_tp // 2
    width = 2 * own_rows
    lows = 2 ** (int(math.log2(n_sp)) // 2)
    highs = n_sp // lows
    slots = chips * n_sp + n_sp * ctx_rows // width
    n_tiles = chips * groups
    split = 2 if width // 2 % 128 == 0 else 1
    bands = columns // 128
    offset = math.log(tok / (2.0 * ctx_rows))
    dma = pltpu.SemaphoreType.DMA
    return pl.pallas_call(
        functools.partial(kernel, n_sp, n_tp, lows, offset, split),
        out_shape=jax.ShapeDtypeStruct(latent.shape, BF16),
        in_specs=[ANY] * 2 + [VMEM] * 3 + [ANY] * 6 + [VMEM] * 2 + [ANY],
        out_specs=VMEM,
        scratch_shapes=[
            pltpu.VMEM((chips, width, model), BF16),
            pltpu.VMEM(context.shape, BF16),
            pltpu.VMEM((3, row_slab, columns), BF16),
            pltpu.VMEM((model, q_width + 2 * kv_width), BF16),
            pltpu.VMEM((2,) + (key_weight.shape if kv_width % 128 else (16, 128)), BF16),
            pltpu.VMEM(output_weight.shape, BF16),
            pltpu.VMEM((4 * bands, 128), F32),
            pltpu.VMEM((n_sp, 4 * bands, 128), F32),
            pltpu.VMEM((n_tp, 4 * bands, 128), F32),
            pltpu.VMEM((8, 128), F32),
            pltpu.VMEM((n_sp, 8, 128), F32),
            pltpu.VMEM((n_tp, 8, 128), F32),
            pltpu.VMEM((8, model), F32),
            pltpu.VMEM((width, model), BF16),
            pltpu.VMEM((chips, SPAN, width), F32),
            pltpu.VMEM((SPAN, width), F32),
            pltpu.VMEM((SPAN, width), F32),
            pltpu.VMEM((chips, groups, heads, SPAN, width), BF16),
            pltpu.VMEM((chips, groups, heads, SPAN, width), BF16),
            pltpu.VMEM((chips, groups, 2 * SPAN, width), BF16),
            pltpu.VMEM((groups, ctx_rows, 2 * SPAN), BF16),
            pltpu.VMEM((n_sp, ctx_rows, 2 * SPAN), BF16),
            pltpu.VMEM((n_tiles, heads, 2 * SPAN, width), BF16),
            pltpu.VMEM((slots, 2 * SPAN + 16, width), BF16),
            pltpu.VMEM((slots, width, 2 * SPAN), BF16),
            pltpu.VMEM((n_tiles, heads, 8, width), F32),
            pltpu.VMEM((n_tiles, heads, SPAN + 16, width), F32),
            pltpu.VMEM((chips, groups, width, 2 * SPAN), BF16),
            pltpu.VMEM((n_tp * groups, own_rows, 2 * SPAN), BF16),
            dma((9,)), dma((chips, PIECES)), dma((max(chips - 1, 1), PIECES)), dma((n_tp, PIECES)),
            dma((2, n_sp - 1)), dma((2, n_sp - 1)), dma((2, n_tp - 1)), dma((2, n_tp - 1)),
            dma((chips, split, max(groups - 1, 1))), dma((chips, split, groups)),
            dma((chips, split, highs - 1)), dma((chips, split, lows - 1)),
            dma((chips, split, highs - 1, lows - 1)), dma((chips, split, n_sp)),
            dma((highs - 1,)), dma((lows - 1,)), dma((highs - 1, lows - 1)), dma((n_sp,)),
            dma((chips, groups, 2)), dma((n_tp * groups,)),
        ],
        compiler_params=pltpu.CompilerParams(
            collective_id=0, has_side_effects=True, vmem_limit_bytes=60 << 20
        ),
        name="fused",
    )(
        latent, context, condition[None], context_condition[None], norm_gain[None],
        shift_weight, scale_weight, gate_weight, query_weight, key_weight, value_weight,
        query_gain[None], key_gain[None], output_weight,
    )


def solution(mesh):
    in_specs = (
        P(("sp", "tp"), None), P("sp", None), P(), P(), P(),
        P("sp", "tp"), P("sp", "tp"), P("sp", "tp"),
        P(None, "tp"), P(None, "tp"), P(None, "tp"), P(), P(), P(),
    )
    return jax.shard_map(
        on_device, mesh=mesh, in_specs=in_specs, out_specs=P(("sp", "tp"), None), check_vma=False
    )
```

time: 59.3 us -> 49 us (0.83)
  Pallas kernels: 57.2 us -> 46.9 us
    pallas_call x1, Pallas kernels: 57.2 us -> 46.9 us  [on_device(): pl.pallas_call(functools.partial(kernel, n_sp, n_tp, lows, offset, split)...]
where the time goes in v2:
time: 49 us; the launch traced here: 48.8 us
  Pallas kernels  46.9 us (96%)
  local copies, waits for them, and re-layouts  1.88 us (4%)
    pallas_call x1, Pallas kernels, on_device(): pl.pallas_call(functools.partial(kernel, n_sp, n_tp, lows, offset, split)...  46.9 us
    unnamed x1, local copies, waits for them, and re-layouts  1.88 us

profile of v2, /device:TPU:0, one launch (start us, length us, event | category | flops | bytes accessed | tf_op | source)
XLA Modules:
  0.0 48.8 jit_solution(7436321181378625609)
XLA Ops:
  0.0 46.9 %fused.1 = bf16[128,2048]{1,0:T(8,128)(2,1)} custom-call(bf16[128,2048]{1,0:T(8,128)(2,1)} %latent_hbm.1, bf16[64,2048]{1,0:T(8,128)(2,1)} %context_hbm.1, f32[1,2048]{1,0:T(1,128)} %bitcast.5, f32[1,2048]{1,0:T(1,128)} %bitcast.6, f32[1,2048]{1,0:T(1,128)} %bitcast.7, bf16[256,512]{1,0:T(8,128)(2,1)} %w_shift_hbm.1, bf16[256,512]{1,0:T(8,128)(2,1)} %w_scale_hbm.1, ...), custom_call_target="tpu_custom_call" | custom-call | tf_op jit(solution)/shard_map/fused/pallas_call | solution.py:654
  46.9 1.9 %copy.16 = bf16[128,2048]{1,0:T(8,128)(2,1)} copy(bf16[128,2048]{1,0:T(8,128)(2,1)} %fused.1) | data formatting | bytes 1048576

commit v3 on v2

--- a/solution.py
+++ b/solution.py
@@ -11,7 +11,8 @@
 SPAN = 64
 GRID_W = 64
 QUARTER = SPAN // 4
-LAG = 6
+LAG = 4
+OWE = 0
 PIECES = 2
 LOG2E = 1.4426950408889634
 MESH = pl.DeviceIdType.MESH
@@ -26,15 +27,15 @@
 
 def kernel(
     n_sp, n_tp, lows, offset, split,
-    latent_hbm, context_hbm, cond, ctx_cond, norm_gain, w_shift_hbm, w_scale_hbm, w_gate_hbm,
-    w_q_hbm, w_k_hbm, w_v_hbm, q_gain, k_gain, w_out_hbm,
-    out,
+    latent_hbm, context_hbm, cond_hbm, ctx_cond_hbm, norm_gain_hbm, w_shift_hbm, w_scale_hbm,
+    w_gate_hbm, w_q_hbm, w_k_hbm, w_v_hbm, q_gain_hbm, k_gain_hbm, w_out_hbm,
+    out, cond, ctx_cond, norm_gain, q_gain, k_gain,
     lat, context, w_mod, w_all, w_side, w_out, part, parts, mods, part_g, parts_g, mods_g,
     coef, hidden, table, gain_q, gain_k, q_send, q_raw, kv_send, ctx_send, ctx_all, q_all, kv_all,
     k_nat, peak, acc, attended, received,
     load, lat_send, lat_fwd, lat_recv, sp_send, sp_recv, tp_send, tp_recv,
     q_ssem, q_rsem, z_send, y_send, f_send, kv_recv,
-    cz_send, cy_send, cf_send, c_recv, at_send, at_recv,
+    cz_send, cy_send, cf_send, c_recv, at_send, at_recv, small_sem,
 ):
     sp, tp = lax.axis_index("sp"), lax.axis_index("tp")
     chips = n_tp // 2
@@ -100,6 +101,17 @@
     else:
         pairs += [(w_k_hbm, w_side.at[0]), (w_v_hbm, w_side.at[1])]
     pairs.append((w_out_hbm, w_out))
+    small = [
+        pltpu.make_async_copy(s, d, small_sem.at[i])
+        for i, (s, d) in enumerate(
+            (
+                (cond_hbm, cond), (ctx_cond_hbm, ctx_cond), (norm_gain_hbm, norm_gain),
+                (q_gain_hbm, q_gain), (k_gain_hbm, k_gain),
+            )
+        )
+    ]
+    for c in small:
+        c.start()
     loads = [pltpu.make_async_copy(s, d, load.at[i]) for i, (s, d) in enumerate(pairs)]
     for c in loads[:-1]:
         c.start()
@@ -115,6 +127,8 @@
             result = jnp.where(pick == k, pltpu.roll(window, 128 - k * row_slab, 1), result)
         return result[:, :row_slab]
 
+    for c in small:
+        c.wait()
     v = jnp.concatenate([slab(cond), slab(ctx_cond)], axis=0)
     act = (v / (1.0 + jnp.exp(-v))).astype(BF16)
     part_g[...] = jnp.zeros_like(part_g)
@@ -245,8 +259,7 @@
 
         lax.fori_loop(0, rows // block, body, 0, unroll=min(4, rows // block))
 
-    far = [d for d in range(2, highs)] if highs > 2 else []
-    z_order = far[:1] + [1] + far[1:] if highs > 1 else []
+    z_order = list(range(highs - 1, 0, -1))
     tail_sends = []
 
     def begin(c):
@@ -361,9 +374,10 @@
                 r = (j * heads + h) * SPAN
                 y = finish(up[r : r + SPAN], gain_q, d, lanes)
                 q_send[d, j, h, :, lanes] = (y * SPAN ** (-0.5)).astype(BF16)
-        for r in range(1, groups):
-            other = lax.rem(g + r, groups)
-            begin(q_copy(d, p, other, q_ssem.at[d, p, r - 1], base + other))
+        if d == 0:
+            for r in range(1, groups):
+                other = lax.rem(g + r, groups)
+                begin(q_copy(d, p, other, q_ssem.at[d, p, r - 1], base + other))
         for dz in z_order:
             z = lax.rem(high + dz, highs)
             src = kv_send.at[d, lax.rem(z, groups), :, lanes]
@@ -372,6 +386,10 @@
             y = lax.rem(low + dl, lows)
             src = kv_send.at[d, g, :, lanes]
             begin(kv_copy(src, d, p, sp, y_send.at[d, p, dl - 1], high, y))
+        if d > 0:
+            for r in range(1, groups):
+                other = lax.rem(g + r, groups)
+                begin(q_copy(d, p, other, q_ssem.at[d, p, r - 1], base + other))
         kv_all[d * n_sp + sp, 0 : 2 * SPAN, lanes] = kv_send[d, g, :, lanes]
         key_rows(d * n_sp + sp, lanes)
 
@@ -423,32 +441,46 @@
             lax.rem(high - dz + highs, highs), lax.rem(low - dl + lows, lows)
         )
 
-    def attend(items):
-        items = [(s, t, h) for s, t in items for h in range(heads)]
-        n = len(items)
-        scores = {}
-
-        def score(i):
-            s, t, h = items[i]
-            r = jnp.dot(k_nat[s], q_all[t, h], preferred_element_type=F32)
-            if isinstance(s, int) and s >= ctx_first:
-                r = r + offset * LOG2E
-            scores[i] = r
-
-        for i in range(min(LAG, n)):
-            score(i)
-        for i in range(n):
-            if i + LAG < n:
-                score(i + LAG)
-            slot, t, h = items[i]
-            s = scores.pop(i)
+    def run(steps):
+        queue, owed = [], []
+
+        def settle(limit):
+            while len(owed) > limit:
+                w, shrink, t, h, action = owed.pop(0)
+                acc[t, h] = acc[t, h] * shrink + w
+                if action is not None:
+                    settle(0)
+                    action()
+
+        def soft():
+            s, slot, t, h, action = queue.pop(0)
             old = peak[t, h, 0:1, :]
             top = jnp.maximum(jnp.max(s, axis=0, keepdims=True), old)
             shrink = jnp.exp2(old - top)
             e = jnp.exp2(s - top).astype(BF16)
             peak[t, h] = jnp.broadcast_to(top, (8, width))
             w = jnp.dot(kv_all[slot, SPAN:, :], e, preferred_element_type=F32)
-            acc[t, h] = acc[t, h] * shrink + w
+            owed.append((w, shrink, t, h, action))
+            settle(OWE)
+
+        for kind, *rest in steps:
+            if kind == "do":
+                rest[0]()
+                continue
+            slot, t, action = rest
+            for h in range(heads):
+                r = jnp.dot(k_nat[slot], q_all[t, h], preferred_element_type=F32)
+                if isinstance(slot, int) and slot >= ctx_first:
+                    r = r + offset * LOG2E
+                queue.append((r, slot, t, h, action if h == heads - 1 else None))
+                if len(queue) > LAG:
+                    soft()
+        while queue:
+            soft()
+        settle(0)
+
+    def attend(items):
+        run([("at", s, t, None) for s, t in items])
 
     def attend_range(first, count, tile_list):
         per = math.gcd(max(1, 8 // len(tile_list)), count)
@@ -529,53 +561,70 @@
         fetch_back(1, 0)
         project(1, 0)
         gate_out = gates()
-        early = [tile_of(0, 0), tile_of(0, 1)]
+        za, zb, zc = z_order
+        own_a, mate_a, own_b, mate_b = (tile_of(d, r) for d in range(2) for r in range(2))
+        early = [own_a, mate_a]
+        ctx = range(ctx_first, ctx_first + ctx_slots)
+        steps = []
+
+        def do(action, *given):
+            steps.append(("do", functools.partial(action, *given)))
+
+        def at(slots, tiles):
+            steps.extend(("at", s, t, None) for s in slots for t in tiles)
+
         q_own(0)
         q_arrive(0)
-        za, zb, zc = z_order
-        attend([(slot_of(0, 0, 0), t) for t in early])
-        column(0, 0, za)
-        column(0, 0, zb)
-        fetch(1, 1)
-        attend([(slot_of(0, dz, 0), t) for dz in (za, zb) for t in early])
-        column(0, 0, zc)
+        at([slot_of(0, 0, 0)], early)
+        do(side, 0, 0, 1)
+        at([slot_of(0, 0, 1)], early)
+        do(column, 0, 0, za)
+        do(fetch, 1, 1)
+        at([slot_of(0, za, 0)], early)
+        do(column, 0, 0, zb)
+        at([slot_of(0, zb, 0)], early)
+        do(fetch_back, 1, 1)
+        do(project, 1, 1)
+        do(q_own, 1)
+        do(column, 0, 0, zc)
         for dz in z_order:
-            ctx_column(dz)
-        fetch_back(1, 1)
-        project(1, 1)
-        q_own(1)
-        side(0, 0, 1)
-        attend([(slot_of(0, zc, 0), t) for t in early] + [(slot_of(0, 0, 1), t) for t in early])
-        column(1, 0, za)
-        side(0, za, 1)
-        side(0, zb, 1)
-        attend([(slot_of(0, dz, 1), t) for dz in (za, zb) for t in early])
-        column(1, 0, zb)
-        column(1, 0, zc)
-        ctx_ready()
-        own_b, mate_b = tile_of(1, 0), tile_of(1, 1)
-        ctx = range(ctx_first, ctx_first + ctx_slots)
-        attend([(s, t) for s in ctx for t in early + [own_b]])
-        column(1, 1, za)
-        side(0, zc, 1)
-        attend(
-            [(slot_of(0, zc, 1), t) for t in early]
-            + [(s, own_b) for s in range(0, n_sp // 2)]
-        )
-        column(1, 1, zb)
-        attend([(s, own_b) for s in range(n_sp // 2, n_sp)])
-        column(1, 1, zc)
-        q_arrive(1)
-        attend([(s, mate_b) for s in list(range(n_sp)) + list(ctx)])
-        every = [tile_of(0, 1), mate_b, own_b, tile_of(0, 0)]
-        attend([(slot_of(1, dz, 0), t) for dz in (0, za) for t in every])
-        attend([(slot_of(1, dz, 0), t) for dz in (zb, zc) for t in every])
-        last = [0] + z_order
-        for dz in last:
-            side(1, dz, 1)
-        for (d, r), t in zip(((0, 1), (1, 1), (1, 0), (0, 0)), every):
-            attend([(slot_of(1, dz, 1), t) for dz in last])
-            deliver(d, r)
+            do(ctx_column, dz)
+        most = early + [own_b]
+        at([slot_of(0, zc, 0), slot_of(1, 0, 0)], most)
+        at([slot_of(0, dz, 0) for dz in (0, za, zb)] + [slot_of(0, 0, 1)], [own_b])
+        do(column, 1, 0, za)
+        do(side, 0, za, 1)
+        at([slot_of(0, za, 1)], most)
+        do(column, 1, 0, zb)
+        do(side, 0, zb, 1)
+        at([slot_of(0, zb, 1)], most)
+        do(ctx_ready)
+        at(ctx, most)
+        do(column, 1, 0, zc)
+        do(side, 0, zc, 1)
+        at([slot_of(0, zc, 1)], most)
+        do(side, 1, 0, 1)
+        at([slot_of(1, 0, 1)], most)
+        do(column, 1, 1, za)
+        at([slot_of(1, za, 0)], most)
+        do(column, 1, 1, zb)
+        do(q_arrive, 1)
+        at(range(n_sp // 2), [mate_b])
+        do(column, 1, 1, zc)
+        at([slot_of(1, zb, 0), slot_of(1, zc, 0)], most)
+        at(range(n_sp // 2, n_sp), [mate_b])
+        at(ctx, [mate_b])
+        at([slot_of(1, dz, 0) for dz in [0] + z_order] + [slot_of(1, 0, 1)], [mate_b])
+        every = [mate_a, mate_b, own_b, own_a]
+        do(side, 1, za, 1)
+        at([slot_of(1, za, 1)], every)
+        do(side, 1, zb, 1)
+        do(side, 1, zc, 1)
+        for place, t in zip(((0, 1), (1, 1), (1, 0), (0, 0)), every):
+            at([slot_of(1, zb, 1)], [t])
+            end = functools.partial(deliver, *place)
+            steps.append(("at", slot_of(1, zc, 1), t, end))
+        run(steps)
     else:
         context_step()
         for d in range(chips):
@@ -651,12 +700,18 @@
     bands = columns // 128
     offset = math.log(tok / (2.0 * ctx_rows))
     dma = pltpu.SemaphoreType.DMA
+
+    def stay(a):
+        return pltpu.with_memory_space_constraint(a, pltpu.HBM)
+
     return pl.pallas_call(
         functools.partial(kernel, n_sp, n_tp, lows, offset, split),
         out_shape=jax.ShapeDtypeStruct(latent.shape, BF16),
-        in_specs=[ANY] * 2 + [VMEM] * 3 + [ANY] * 6 + [VMEM] * 2 + [ANY],
+        in_specs=[ANY] * 14,
         out_specs=VMEM,
         scratch_shapes=[
+            pltpu.VMEM((1, model), F32), pltpu.VMEM((1, model), F32), pltpu.VMEM((1, model), F32),
+            pltpu.VMEM((1, SPAN), F32), pltpu.VMEM((1, SPAN), F32),
             pltpu.VMEM((chips, width, model), BF16),
             pltpu.VMEM(context.shape, BF16),
             pltpu.VMEM((3, row_slab, columns), BF16),
@@ -692,16 +747,18 @@
             dma((chips, split, highs - 1)), dma((chips, split, lows - 1)),
             dma((chips, split, highs - 1, lows - 1)), dma((chips, split, n_sp)),
             dma((highs - 1,)), dma((lows - 1,)), dma((highs - 1, lows - 1)), dma((n_sp,)),
-            dma((chips, groups, 2)), dma((n_tp * groups,)),
+            dma((chips, groups, 2)), dma((n_tp * groups,)), dma((5,)),
         ],
         compiler_params=pltpu.CompilerParams(
-            collective_id=0, has_side_effects=True, vmem_limit_bytes=60 << 20
+            collective_id=0, has_side_effects=True, vmem_limit_bytes=46 << 20
         ),
         name="fused",
     )(
-        latent, context, condition[None], context_condition[None], norm_gain[None],
-        shift_weight, scale_weight, gate_weight, query_weight, key_weight, value_weight,
-        query_gain[None], key_gain[None], output_weight,
+        stay(latent), stay(context), stay(condition[None]), stay(context_condition[None]),
+        stay(norm_gain[None]),
+        stay(shift_weight), stay(scale_weight), stay(gate_weight), stay(query_weight),
+        stay(key_weight), stay(value_weight), stay(query_gain[None]), stay(key_gain[None]),
+        stay(output_weight),
     )
 
 

time: 49 us -> 45.6 us (0.931)
  Pallas kernels: 46.9 us -> 44.7 us
  local copies, waits for them, and re-layouts: 1.88 us -> 0.8 us
    pallas_call x1, Pallas kernels: 46.9 us -> 44.7 us  [on_device(): pl.pallas_call(functools.partial(kernel, n_sp, n_tp, lows, offset, split)...]
    unnamed x1, local copies, waits for them, and re-layouts: 1.88 us -> 0.8 us
where the time goes in v3:
time: 45.6 us; the launch traced here: 45.5 us
  Pallas kernels  44.7 us (98%)
  local copies, waits for them, and re-layouts  0.8 us (2%)
    pallas_call x1, Pallas kernels, on_device(): pl.pallas_call(functools.partial(kernel, n_sp, n_tp, lows, offset, split)...  44.7 us

profile of v3, /device:TPU:0, one launch (start us, length us, event | category | flops | bytes accessed | tf_op | source)
XLA Modules:
  0.0 45.5 jit_solution(9662208542856203899)
XLA Ops:
  0.0 44.7 %fused.1 = bf16[128,2048]{1,0:T(8,128)(2,1)S(1)} custom-call(bf16[128,2048]{1,0:T(8,128)(2,1)} %latent_hbm.1, bf16[64,2048]{1,0:T(8,128)(2,1)} %context_hbm.1, f32[1,2048]{1,0:T(1,128)} %bitcast.5, f32[1,2048]{1,0:T(1,128)} %bitcast.6, f32[1,2048]{1,0:T(1,128)} %bitcast.7, bf16[256,512]{1,0:T(8,128)(2,1)} %w_shift_hbm.1, bf16[256,512]{1,0:T(8,128)(2,1)} %w_scale_hbm.1, ...), custom_call_target="tpu_custom_call" | custom-call | tf_op jit(solution)/shard_map/fused/pallas_call | solution.py:707
  44.7 0.8 %copy.16 = bf16[128,2048]{1,0:T(8,128)(2,1)} copy(bf16[128,2048]{1,0:T(8,128)(2,1)S(1)} %fused.1) | data formatting | bytes 1048576

commit v4 on v3

--- a/solution.py
+++ b/solution.py
@@ -11,7 +11,7 @@
 SPAN = 64
 GRID_W = 64
 QUARTER = SPAN // 4
-LAG = 4
+LAG = 5
 OWE = 0
 PIECES = 2
 LOG2E = 1.4426950408889634
@@ -35,7 +35,7 @@
     k_nat, peak, acc, attended, received,
     load, lat_send, lat_fwd, lat_recv, sp_send, sp_recv, tp_send, tp_recv,
     q_ssem, q_rsem, z_send, y_send, f_send, kv_recv,
-    cz_send, cy_send, cf_send, c_recv, at_send, at_recv, small_sem,
+    cz_send, cy_send, cf_send, c_recv, at_send, at_recv, small_sem, summed_out, inverse,
 ):
     sp, tp = lax.axis_index("sp"), lax.axis_index("tp")
     chips = n_tp // 2
@@ -236,6 +236,15 @@
         w_all[:, q_width:] = jnp.concatenate([w_side[0], w_side[1]], axis=1)
     for piece in range(PIECES):
         row_copy(twin, piece, lat_send.at[0, 0], twin).wait_recv()
+
+    def measure(i, carry):
+        r = pl.ds(pl.multiple_of(i * 16, 16), 16)
+        w = lat[x, r, :].astype(F32)
+        inv = lax.rsqrt(jnp.sum(w * w, axis=-1, keepdims=True) / model + epsilon)
+        inverse[r, :] = jnp.broadcast_to(inv, (16, 128))
+        return carry
+
+    lax.fori_loop(0, width // 16, measure, 0, unroll=4)
     for c in tp_copies:
         c.wait()
     for t in range(n_tp):
@@ -249,17 +258,22 @@
 
     block = 16
 
-    def modulate(read, rows, first, row):
+    def modulate(read, rows, first, row, known=False):
         def body(i, carry):
             w = read(i * block).astype(F32)
-            inv = lax.rsqrt(jnp.sum(w * w, axis=-1, keepdims=True) / model + epsilon)
+            if known:
+                r = pl.ds(pl.multiple_of(i * block, block), block)
+                inv = jnp.concatenate([inverse[r, :]] * (model // 128), axis=1)
+            else:
+                inv = lax.rsqrt(jnp.sum(w * w, axis=-1, keepdims=True) / model + epsilon)
             y = w * inv * coef[row : row + 1, :] + coef[2 + row : 3 + row, :]
             hidden[pl.ds(pl.multiple_of(first + i * block, block), block), :] = y.astype(BF16)
             return carry
 
         lax.fori_loop(0, rows // block, body, 0, unroll=min(4, rows // block))
 
-    z_order = list(range(highs - 1, 0, -1))
+    z_order = [d for d in range(1, highs)]
+    z_order = z_order[1:2] + z_order[:1] + z_order[2:]
     tail_sends = []
 
     def begin(c):
@@ -354,7 +368,7 @@
         n = lanes.stop - lanes.start
         if n == width:
             modulate(
-                lambda i: lat[chip, pl.ds(pl.multiple_of(i, block), block), :], width, 0, 0
+                lambda i: lat[chip, pl.ds(pl.multiple_of(i, block), block), :], width, 0, 0, d == 0
             )
         else:
             for half in range(2):
@@ -608,12 +622,12 @@
         do(column, 1, 1, za)
         at([slot_of(1, za, 0)], most)
         do(column, 1, 1, zb)
+        at([slot_of(1, zb, 0)], most)
+        do(column, 1, 1, zc)
         do(q_arrive, 1)
-        at(range(n_sp // 2), [mate_b])
-        do(column, 1, 1, zc)
-        at([slot_of(1, zb, 0), slot_of(1, zc, 0)], most)
-        at(range(n_sp // 2, n_sp), [mate_b])
+        at(range(n_sp), [mate_b])
         at(ctx, [mate_b])
+        at([slot_of(1, zc, 0)], most)
         at([slot_of(1, dz, 0) for dz in [0] + z_order] + [slot_of(1, 0, 1)], [mate_b])
         every = [mate_a, mate_b, own_b, own_a]
         do(side, 1, za, 1)
@@ -659,21 +673,31 @@
     loads[-1].wait()
     for c in gate_out:
         c.wait()
-    for rt in range(n_tp):
+    order = [tp, twin]
+    for d in range(1, chips):
+        order += [lax.rem(tp + 2 * d, n_tp), lax.rem(twin + 2 * d, n_tp)]
+    for n, src in enumerate(order):
         for r in range(groups):
-            if rt == 0 and r == 0:
+            if n == 0 and r == 0:
                 continue
-            who = lax.rem(tp + rt, n_tp) * groups + lax.rem(g + r, groups)
+            who = src * groups + lax.rem(g + r, groups)
             remote(
                 received.at[who], received.at[who], at_send.at[0, 0, 1], at_recv.at[who],
                 (sp, twin),
             ).wait_recv()
-    rows = jnp.concatenate([received[s] for s in range(n_tp * groups)], axis=1)
-    for t in range(n_tp):
-        cols = slice(t * columns, (t + 1) * columns)
-        gate = jnp.concatenate([mods_g[t, k : k + 1, :] for k in range(bands)], axis=1)
-        branch = jnp.dot(rows, w_out[:, cols], preferred_element_type=F32)
-        out[:, cols] = (lat[x, mine_rows, cols].astype(F32) + gate * branch).astype(BF16)
+        depth = groups * 2 * SPAN
+        rows = jnp.concatenate([received[src * groups + j] for j in range(groups)], axis=1)
+        heights = pl.ds(pl.multiple_of(src * depth, depth), depth)
+        for t in range(n_tp):
+            cols = slice(t * columns, (t + 1) * columns)
+            branch = jnp.dot(rows, w_out[heights, cols], preferred_element_type=F32)
+            if n > 0:
+                branch = branch + summed_out[:, cols]
+            if n < len(order) - 1:
+                summed_out[:, cols] = branch
+            else:
+                gate = jnp.concatenate([mods_g[t, k : k + 1, :] for k in range(bands)], axis=1)
+                out[:, cols] = (lat[x, mine_rows, cols].astype(F32) + gate * branch).astype(BF16)
     for c in lat_sends + tail_sends + copies:
         c.wait_send()
 
@@ -748,6 +772,7 @@
             dma((chips, split, highs - 1, lows - 1)), dma((chips, split, n_sp)),
             dma((highs - 1,)), dma((lows - 1,)), dma((highs - 1, lows - 1)), dma((n_sp,)),
             dma((chips, groups, 2)), dma((n_tp * groups,)), dma((5,)),
+            pltpu.VMEM(latent.shape, F32), pltpu.VMEM((width, 128), F32),
         ],
         compiler_params=pltpu.CompilerParams(
             collective_id=0, has_side_effects=True, vmem_limit_bytes=46 << 20

time: 45.6 us -> 44.6 us (0.978)
  Pallas kernels: 44.7 us -> 43.7 us
    pallas_call x1, Pallas kernels: 44.7 us -> 43.7 us  [on_device(): pl.pallas_call(functools.partial(kernel, n_sp, n_tp, lows, offset, split)...]
where the time goes in v4:
time: 44.6 us; the launch traced here: 44.5 us
  Pallas kernels  43.7 us (98%)
  local copies, waits for them, and re-layouts  0.8 us (2%)
    pallas_call x1, Pallas kernels, on_device(): pl.pallas_call(functools.partial(kernel, n_sp, n_tp, lows, offset, split)...  43.7 us

profile of v4, /device:TPU:0, one launch (start us, length us, event | category | flops | bytes accessed | tf_op | source)
XLA Modules:
  0.0 44.5 jit_solution(16895742353838286135)
XLA Ops:
  0.0 43.7 %fused.1 = bf16[128,2048]{1,0:T(8,128)(2,1)S(1)} custom-call(bf16[128,2048]{1,0:T(8,128)(2,1)} %latent_hbm.1, bf16[64,2048]{1,0:T(8,128)(2,1)} %context_hbm.1, f32[1,2048]{1,0:T(1,128)} %bitcast.5, f32[1,2048]{1,0:T(1,128)} %bitcast.6, f32[1,2048]{1,0:T(1,128)} %bitcast.7, bf16[256,512]{1,0:T(8,128)(2,1)} %w_shift_hbm.1, bf16[256,512]{1,0:T(8,128)(2,1)} %w_scale_hbm.1, ...), custom_call_target="tpu_custom_call" | custom-call | tf_op jit(solution)/shard_map/fused/pallas_call | solution.py:731
  43.7 0.8 %copy.16 = bf16[128,2048]{1,0:T(8,128)(2,1)} copy(bf16[128,2048]{1,0:T(8,128)(2,1)S(1)} %fused.1) | data formatting | bytes 1048576

commit v5 on v4

--- a/solution.py
+++ b/solution.py
@@ -601,22 +601,22 @@
         do(project, 1, 1)
         do(q_own, 1)
         do(column, 0, 0, zc)
-        for dz in z_order:
-            do(ctx_column, dz)
         most = early + [own_b]
         at([slot_of(0, zc, 0), slot_of(1, 0, 0)], most)
         at([slot_of(0, dz, 0) for dz in (0, za, zb)] + [slot_of(0, 0, 1)], [own_b])
+        for dz in z_order:
+            do(ctx_column, dz)
         do(column, 1, 0, za)
         do(side, 0, za, 1)
         at([slot_of(0, za, 1)], most)
         do(column, 1, 0, zb)
         do(side, 0, zb, 1)
         at([slot_of(0, zb, 1)], most)
-        do(ctx_ready)
-        at(ctx, most)
         do(column, 1, 0, zc)
         do(side, 0, zc, 1)
         at([slot_of(0, zc, 1)], most)
+        do(ctx_ready)
+        at(ctx, most)
         do(side, 1, 0, 1)
         at([slot_of(1, 0, 1)], most)
         do(column, 1, 1, za)

time: 44.6 us -> 44.1 us (0.989)
  Pallas kernels: 43.7 us -> 43.1 us
    pallas_call x1, Pallas kernels: 43.7 us -> 43.1 us  [on_device(): pl.pallas_call(functools.partial(kernel, n_sp, n_tp, lows, offset, split)...]
where the time goes in v5:
time: 44.1 us; the launch traced here: 43.9 us
  Pallas kernels  43.1 us (98%)
  local copies, waits for them, and re-layouts  0.8 us (2%)
    pallas_call x1, Pallas kernels, on_device(): pl.pallas_call(functools.partial(kernel, n_sp, n_tp, lows, offset, split)...  43.1 us

profile of v5, /device:TPU:0, one launch (start us, length us, event | category | flops | bytes accessed | tf_op | source)
XLA Modules:
  0.0 43.9 jit_solution(16252905652632830773)
XLA Ops:
  0.0 43.1 %fused.1 = bf16[128,2048]{1,0:T(8,128)(2,1)S(1)} custom-call(bf16[128,2048]{1,0:T(8,128)(2,1)} %latent_hbm.1, bf16[64,2048]{1,0:T(8,128)(2,1)} %context_hbm.1, f32[1,2048]{1,0:T(1,128)} %bitcast.5, f32[1,2048]{1,0:T(1,128)} %bitcast.6, f32[1,2048]{1,0:T(1,128)} %bitcast.7, bf16[256,512]{1,0:T(8,128)(2,1)} %w_shift_hbm.1, bf16[256,512]{1,0:T(8,128)(2,1)} %w_scale_hbm.1, ...), custom_call_target="tpu_custom_call" | custom-call | tf_op jit(solution)/shard_map/fused/pallas_call | solution.py:731
  43.1 0.8 %copy.16 = bf16[128,2048]{1,0:T(8,128)(2,1)} copy(bf16[128,2048]{1,0:T(8,128)(2,1)S(1)} %fused.1) | data formatting | bytes 1048576
